TPU v7x, 256 devices: a whole 4x4x8 slice. The times are simulated.
256 devices in a mesh: fs: 64 (over z, x, core), tp: 4 (over y).
Axes of the slice: x: 4, y: 4, z: 8, core: 2. Of those that a mesh axis runs over, the one named last changes fastest.
Arguments:
- inputs: bfloat16 [24576, 2048], P('fs'), may hold values from -6 to 6
- queries: bfloat16 [24576, 2048], P('fs', 'tp'), may hold values from -6 to 6
- keys: bfloat16 [24576, 2048], P('fs', 'tp'), may hold values from -6 to 6
- values: bfloat16 [24576, 2048], P('fs', 'tp'), may hold values from -6 to 6
- head_cot: bfloat16 [24576, 2048], P('fs', 'tp'), may hold values from -6 to 6
- mixing: float32 [16], P('tp'), may hold values from 0.3 to 0.8
- head_gain: float32 [128], replicated, may hold values from 0.1 to 1.9
- factors: bfloat16 [2048, 2, 256], P('fs'), may hold values from -0.375 to 0.375
- moments: float32 [256, 2, 2048], P('fs', None, 'tp'), may hold values from -6 to 6
- weights: float32 [2048, 2, 2048], P('fs', None, 'tp'), may hold values from -6 to 6
Outputs:
- step: float32 [2048, 2, 2048], P('fs', None, 'tp')
- new_moments: float32 [256, 2, 2048], P('fs', None, 'tp')
- copies: bfloat16 [2048, 2, 2048], P(None, None, 'tp')
All inputs are finite; a program needn't handle non-finite values.
Results may differ from a plain program's by a relative error of at most 0.007.
Values may be sent and summed in bfloat16 or wider, within the bound.
No kernel may reach another device: no remote copies, remote signals or barrier semaphores. Data moves between devices by JAX's collectives and lax.ppermute only.
A program may use at most 64 MiB of HBM per device.

v0:
```python
import jax
import jax.numpy as jnp
from jax import lax
from jax.sharding import Mesh
from jax.sharding import PartitionSpec as P

FS = ("fs_0", "fs_1", "fs_2")
FS_TP = ("fs_0", "fs_1", "fs_2", "tp")


EPS = 0.05
BETA = 0.9
RATE_BASE = 0.5


def sent_to_all(shard, axis):
    copies = jnp.broadcast_to(shard, (lax.axis_size(axis), *shard.shape))
    return lax.all_to_all(copies, axis, split_axis=0, concat_axis=0, tiled=True)


def joined_along(parts, dim):
    parts = jnp.moveaxis(parts, 0, dim)
    lengths = parts.shape
    return parts.reshape(*lengths[:dim], lengths[dim] * lengths[dim + 1], *lengths[dim + 2 :])


def collect(shard, axis, dim):
    parts = sent_to_all(shard, axis)
    return joined_along(parts, dim)


def in_blocks(shard, dim, length):
    lengths = shard.shape
    parts = shard.reshape(*lengths[:dim], length, lengths[dim] // length, *lengths[dim + 1 :])
    return jnp.moveaxis(parts, dim, 0)


def sum_at_owner(shard, axis, dim):
    length = lax.axis_size(axis)
    parts = lax.all_to_all(in_blocks(shard, dim, length), axis, 0, 0, tiled=True)
    return jnp.sum(parts, axis=0)


def by_axis(shard, axes):
    for axis in axes:
        shard = lax.psum(shard, axis)
    return shard


def softmax_rows(scores):
    top = jnp.max(scores, axis=-1, keepdims=True)
    expo = jnp.exp(scores - top)
    return expo / jnp.sum(expo, axis=-1, keepdims=True)


def head_grads(query, key_rows, value, upstream, weight_mix, head_gain):
    length = query.shape[0]
    head_dim = query.shape[2]
    factor = head_dim ** (-0.5)
    places = jnp.arange(length)
    causal = places[None, :] <= places[:, None]

    def probs(which):
        scores = (
            jnp.dot(query[:, which], key_rows[:, which].T, preferred_element_type=jnp.float32)
            * factor
        )
        return softmax_rows(jnp.where(causal, scores, -jnp.inf))

    first = probs(0)
    second = probs(1)
    mixed = (first - weight_mix * second).astype(jnp.bfloat16)
    output = jnp.dot(mixed, value, preferred_element_type=jnp.float32)
    inverse = lax.rsqrt(jnp.mean(output * output, axis=-1, keepdims=True) + EPS)
    scaled = head_gain * upstream.astype(jnp.float32)
    d_out = inverse * scaled - output * inverse**3 * jnp.mean(
        output * scaled, axis=-1, keepdims=True
    )
    d_out = d_out.astype(jnp.bfloat16)
    d_value = jnp.dot(mixed.T, d_out, preferred_element_type=jnp.float32).astype(jnp.bfloat16)
    d_mix = jnp.dot(d_out, value.T, preferred_element_type=jnp.float32)
    d_first = (first * (d_mix - jnp.sum(first * d_mix, axis=-1, keepdims=True))).astype(
        jnp.bfloat16
    )
    d_second = (
        -weight_mix * second * (d_mix - jnp.sum(second * d_mix, axis=-1, keepdims=True))
    ).astype(jnp.bfloat16)
    q_first = (
        jnp.dot(d_first, key_rows[:, 0], preferred_element_type=jnp.float32) * factor
    ).astype(jnp.bfloat16)
    q_second = (
        jnp.dot(d_second, key_rows[:, 1], preferred_element_type=jnp.float32) * factor
    ).astype(jnp.bfloat16)
    return (jnp.stack([q_first, q_second], axis=1).reshape(length, 2 * head_dim), d_value)


def per_device(
    inputs, queries, keys, values, head_cot, mixing, head_gain, factors, moments, weights
):
    length = inputs.shape[0]
    heads_here = mixing.shape[0]
    head_width = values.shape[1] // heads_here
    head_dim = head_width // 2
    query_heads = queries.reshape(length, heads_here, 2, head_dim).transpose(1, 0, 2, 3)
    key_heads = keys.reshape(length, heads_here, 2, head_dim).transpose(1, 0, 2, 3)
    value_heads = values.reshape(length, heads_here, head_width).transpose(1, 0, 2)
    upstream_heads = head_cot.reshape(length, heads_here, head_width).transpose(1, 0, 2)

    def one_head(pieces):
        return head_grads(pieces[0], pieces[1], pieces[2], pieces[3], pieces[4], head_gain)

    d_query, d_value = lax.map(
        one_head, (query_heads, key_heads, value_heads, upstream_heads, mixing)
    )
    d_query = d_query.transpose(1, 0, 2).reshape(length, heads_here * head_width)
    d_value = d_value.transpose(1, 0, 2).reshape(length, heads_here * head_width)
    cotangents = jnp.stack([d_query, d_value], axis=1)
    fs_count = lax.axis_size(FS)
    token_factor = (length * fs_count) ** (-0.5)
    rank_here = moments.shape[0]
    cols_here = moments.shape[2]
    factor_wide = factors.astype(jnp.float32)
    whole_factors = collect(factors, FS, 0)
    reduced = jnp.einsum("td,dkr->tkr", inputs, whole_factors, preferred_element_type=jnp.float32)
    reduced_upper = reduced.astype(jnp.bfloat16)
    reduced_lower = (reduced - reduced_upper.astype(jnp.float32)).astype(jnp.bfloat16)
    upper_part = jnp.einsum(
        "tkr,tke->rke", reduced_upper, cotangents, preferred_element_type=jnp.float32
    )
    lower_part = jnp.einsum(
        "tkr,tke->rke", reduced_lower, cotangents, preferred_element_type=jnp.float32
    )
    projected = sum_at_owner(upper_part + lower_part, FS, 0)
    projected = projected * token_factor
    new_moments = BETA * moments + projected
    local_sums = jnp.sum(new_moments * new_moments, axis=(0, 2))
    totals = by_axis(local_sums, FS_TP)
    entries = rank_here * fs_count * cols_here * lax.axis_size("tp")
    rate = RATE_BASE / jnp.sqrt(1.0 + totals / entries)
    low_part = jnp.einsum("dkr,rke->dke", factor_wide, collect(new_moments, FS, 0))
    step = low_part * rate[None, :, None]
    copies = lax.all_gather((weights - step).astype(jnp.bfloat16), FS, axis=0, tiled=True)
    return (step, new_moments, copies)


def solution(mesh):
    torus = Mesh(mesh.devices.reshape(8, 4, 2, mesh.shape["tp"]), ("fs_0", "fs_1", "fs_2", "tp"))
    placed = (
        P(FS, None),
        P(FS, "tp"),
        P(FS, "tp"),
        P(FS, "tp"),
        P(FS, "tp"),
        P("tp"),
        P(),
        P(FS, None, None),
        P(FS, None, "tp"),
        P(FS, None, "tp"),
    )
    return jax.shard_map(
        per_device,
        mesh=torus,
        in_specs=placed,
        out_specs=(P(FS, None, "tp"), P(FS, None, "tp"), P(None, None, "tp")),
        check_vma=False,
    )
```

profile of v0, /device:TPU:2, one launch (start us, length us, event | category | flops | bytes accessed | tf_op | source)
XLA Modules:
  0.0 260.3 jit_solution(12092849654604875013)
XLA Ops:
  7.2 0.9 copy.50
  8.1 1.6 broadcast_in_dim.27
  9.7 12.3 %all-to-all-start = ((bf16[64,32,2,256]{3,1,2,0:T(8,128)(2,1)}), bf16[64,32,2,256]{3,1,2,0:T(8,128)(2,1)}, u32[]{:S(2)}, u32[]{:S(2)}) async-start(bf16[64,32,2,256]{3,1,2,0:T(8,128)(2,1)} %broadcast_in_dim.27), calls=%async_computation | async-start | bytes 4194304 | tf_op jit(solution)/shard_map/all_to_all | solution.py:18
  23.2 23.9 %while.12 = (s32[]{:T(128)}, bf16[4,384,128]{1,2,0:T(8,128)(2,1)}, bf16[4,384,128]{2,1,0:T(8,128)(2,1)}, bf16[4,384,2,64]{1,3,2,0:T(8,128)(2,1)S(1)}, bf16[4,384...) while((s32[]{:T(128)}, bf16[4,384,128]{1,2,0:T(8,128)(2,1)}, ...), condition=%wide.region_9.10_spmd, body=%wide.region_0.9_spmd.sunk | while | flops 195525504 | bytes 10978449 | solution.py:112
  23.2 0.6 dynamic_slice.47
  25.4 0.9 subtract_convert_fusion.4
  26.5 1.0 fusion.72
  27.5 0.4 multiply_reduce_fusion.7
  28.6 0.7 constant_dynamic-update-slice_fusion.2
  29.2 0.6 dynamic_slice.47
  30.9 0.3 fusion.66
  31.4 0.9 subtract_convert_fusion.4
  32.5 1.0 fusion.72
  33.5 0.4 multiply_reduce_fusion.7
  34.5 0.7 constant_dynamic-update-slice_fusion.2
  35.2 0.6 dynamic_slice.47
  36.9 0.3 fusion.66
  37.3 0.9 subtract_convert_fusion.4
  38.5 1.0 fusion.72
  39.4 0.4 multiply_reduce_fusion.7
  40.5 0.7 constant_dynamic-update-slice_fusion.2
  41.1 0.6 dynamic_slice.47
  42.9 0.3 fusion.66
  43.3 0.9 subtract_convert_fusion.4
  44.4 1.0 fusion.72
  45.4 0.4 multiply_reduce_fusion.7
  46.5 0.6 constant_dynamic-update-slice_fusion.2
  47.1 1.3 copy.49
  48.6 1.2 copy.64
  49.8 23.4 %all-to-all-done = bf16[64,32,2,256]{3,1,2,0:T(8,128)(2,1)} async-done(((bf16[64,32,2,256]{3,1,2,0:T(8,128)(2,1)}), bf16[64,32,2,256]{3,1,2,0:T(8,128)(2,1)}, u32[]{:S(2)}, u32[]{:S(2)}) %all-to-all-start) | async-done | bytes 2097184 | tf_op jit(solution)/shard_map/all_to_all | solution.py:18
  73.1 1.8 copy.51
  74.9 1.0 fusion.30
  75.9 0.5 fusion.34
  76.4 0.5 fusion.32
  76.9 1.3 reshape.62
  78.2 1.4 copy.54
  79.6 34.1 %all_to_all.15 = f32[64,4,2,512]{3,1,2,0:T(4,128)S(1)} all-to-all(f32[64,4,2,512]{3,1,2,0:T(4,128)S(1)} %copy.54), channel_id=1, replica_groups=mesh['fs_0'=8,'fs_1'=4,'fs_2'=2,'tp'=4] {'fs_0','fs_1','fs_2'}, dimensions={0} | all-to-all | bytes 2097152 | tf_op jit(solution)/shard_map/all_to_all | solution.py:40
  114.0 0.9 broadcast_in_dim.28
  115.0 5.7 %all-to-all-start.2 = ((bf16[64,4,2,512]{3,1,2,0:T(4,128)(2,1)}), bf16[64,4,2,512]{3,1,2,0:T(4,128)(2,1)S(1)}, u32[]{:S(2)}, u32[]{:S(2)}) async-start(bf16[64,4,2,512]{3,1,2,0:T(4,128)(2,1)} %broadcast_in_dim.28), calls=%async_computation.2 | async-start | bytes 1048576 | tf_op jit(solution)/shard_map/all_to_all | solution.py:18
  120.7 24.1 %psum.28 = f32[2]{0:T(128)S(1)} all-reduce(f32[2]{0:T(128)S(1)} %get-tuple-element.111), channel_id=1, replica_groups=mesh['fs_0'=8,'fs_1'=4,'fs_2'=2,'tp'=4] {'fs_0'}, use_global_device_ids=true, to_apply=%region_12.13 | all-reduce | flops 2 | bytes 16 | tf_op jit(solution)/shard_map/psum | solution.py:46
  144.8 8.5 %psum.29 = f32[2]{0:T(128)S(1)} all-reduce(f32[2]{0:T(128)S(1)} %psum.28), channel_id=1, replica_groups=mesh['fs_0'=8,'fs_1'=4,'fs_2'=2,'tp'=4] {'fs_1'}, use_global_device_ids=true, to_apply=%region_13.14 | all-reduce | flops 2 | bytes 16 | tf_op jit(solution)/shard_map/psum | solution.py:46
  153.3 2.5 psum.30
  155.8 10.7 %psum.31 = f32[2]{0:T(128)S(1)} all-reduce(f32[2]{0:T(128)S(1)} %psum.30), channel_id=1, replica_groups=mesh['fs_0'=8,'fs_1'=4,'fs_2'=2,'tp'=4] {'tp'}, use_global_device_ids=true, to_apply=%region_15.16 | all-reduce | flops 2 | bytes 16 | tf_op jit(solution)/shard_map/psum | solution.py:46
  166.9 0.8 fusion.37
  167.7 0.6 copy.60
  168.3 0.8 copy.59
  169.1 74.3 %all-gather.2.cloned.1.call-done = bf16[2048,2,512]{2,0,1:T(8,128)(2,1)} async-done(((bf16[32,2,512]{2,0,1:T(8,128)(2,1)}), bf16[2048,2,512]{2,0,1:T(8,128)(2,1)}) %all-gather.2.cloned.1.call-update) | async-done | bytes 4194320 | tf_op jit(solution)/shard_map/all_gather | solution.py:142
  243.4 10.1 %copy.61 = bf16[2048,2,512]{2,1,0:T(2,128)(2,1)} copy(bf16[2048,2,512]{2,0,1:T(8,128)(2,1)} %all-gather.2.cloned.1.call-done) | data formatting | bytes 8388608
  (76 shorter events, 8.1 us)
Async XLA Ops:
  7.2 67.8 %copy-start = (bf16[384,2048]{1,0:T(8,128)(2,1)S(1)}, bf16[384,2048]{1,0:T(8,128)(2,1)}, u32[]{:S(2)}) copy-start(bf16[384,2048]{1,0:T(8,128)(2,1)} %param.12) | copy-start | bytes 4718596
  9.6 12.4 %copy-start.1 = (bf16[384,512]{1,0:T(8,128)(2,1)S(1)}, bf16[384,512]{1,0:T(8,128)(2,1)}, u32[]{:S(2)}) copy-start(bf16[384,512]{1,0:T(8,128)(2,1)} %param.13) | copy-start | bytes 1179652
  9.6 12.6 %copy-start.2 = (bf16[384,512]{1,0:T(8,128)(2,1)S(1)}, bf16[384,512]{1,0:T(8,128)(2,1)}, u32[]{:S(2)}) copy-start(bf16[384,512]{1,0:T(8,128)(2,1)} %param.14) | copy-start | bytes 1179652
  9.6 12.9 %copy-start.3 = (bf16[384,512]{1,0:T(8,128)(2,1)S(1)}, bf16[384,512]{1,0:T(8,128)(2,1)}, u32[]{:S(2)}) copy-start(bf16[384,512]{1,0:T(8,128)(2,1)} %param.15) | copy-start | bytes 1179652
  9.7 63.5 %all-to-all-start = ((bf16[64,32,2,256]{3,1,2,0:T(8,128)(2,1)}), bf16[64,32,2,256]{3,1,2,0:T(8,128)(2,1)}, u32[]{:S(2)}, u32[]{:S(2)}) async-start(bf16[64,32,2,256]{3,1,2,0:T(8,128)(2,1)} %broadcast_in_dim.27), calls=%async_computation | async-start | bytes 4194304 | tf_op jit(solution)/shard_map/all_to_all | solution.py:18
  22.0 1.0 copy-start.4
  22.0 1.2 copy-start.7
  22.0 1.2 copy-start.9
  79.6 34.3 %copy-start.8 = (f32[4,2,512]{2,1,0:T(2,128)S(1)}, f32[4,2,512]{2,1,0:T(2,128)}, u32[]{:S(2)}) copy-start(f32[4,2,512]{2,1,0:T(2,128)} %param.20) | copy-start | bytes 49156
  113.9 52.9 %copy-start.5 = (bf16[32,2,256]{2,1,0:T(2,128)(2,1)S(1)}, bf16[32,2,256]{2,1,0:T(2,128)(2,1)}, u32[]{:S(2)}) copy-start(bf16[32,2,256]{2,1,0:T(2,128)(2,1)} %param.19) | copy-start | bytes 98308
  113.9 52.9 %copy-start.6 = (f32[32,2,512]{2,1,0:T(2,128)S(1)}, f32[32,2,512]{2,1,0:T(2,128)}, u32[]{:S(2)}) copy-start(f32[32,2,512]{2,1,0:T(2,128)} %param.21) | copy-start | bytes 393220
  115.0 51.5 %all-to-all-start.2 = ((bf16[64,4,2,512]{3,1,2,0:T(4,128)(2,1)}), bf16[64,4,2,512]{3,1,2,0:T(4,128)(2,1)S(1)}, u32[]{:S(2)}, u32[]{:S(2)}) async-start(bf16[64,4,2,512]{3,1,2,0:T(4,128)(2,1)} %broadcast_in_dim.28), calls=%async_computation.2 | async-start | bytes 1048576 | tf_op jit(solution)/shard_map/all_to_all | solution.py:18
  120.7 122.7 %all-gather.2.cloned.1.call-start = ((), (), s32[]{:S(2)}) async-start(), calls=%async_computation.3 | async-start | bytes 4259840 | tf_op jit(solution)/shard_map/all_gather | solution.py:142
Sparse Core Ops, SparseCore 0:
  167.8 75.5 all-gather.1
where the time goes:
time: 264 us; the launch traced here: 260 us
  waiting for transfers between devices  97.7 us (37%)
  blocking collectives  79.9 us (30%)
  local copies, waits for them, and re-layouts  28.4 us (11%)
  starting transfers between devices  18 us (7%)
  between operations  14.3 us (5%)
  matrix products  14.2 us (5%)
  other arithmetic  4.92 us (2%)
  loops' own time  2.83 us (1%)
    all_gather x1, waiting for transfers between devices, per_device(): lax.all_gather((weights - step).astype(jnp.bfloat16), FS, axis=0, tiled=T...  74.3 us
    psum x4, blocking collectives, by_axis(): shard = lax.psum(shard, axis)  45.8 us
    all_to_all x1, blocking collectives, sum_at_owner(): lax.all_to_all(in_blocks(shard, dim, length), axis, 0, 0, tiled=True)  34.1 us
    all_to_all x2, waiting for transfers between devices, sent_to_all(): return lax.all_to_all(copies, axis, split_axis=0, concat_axis=0, tiled=True)  23.4 us
    all_to_all x2, starting transfers between devices, sent_to_all(): return lax.all_to_all(copies, axis, split_axis=0, concat_axis=0, tiled=True)  18 us
    unnamed x28, local copies, waits for them, and re-layouts  13.5 us
  transfers between devices with their start and end apart: 3, of which 2 were waited for; matrix products, arithmetic and copies ran while one was open for 10% of the time, Pallas kernels for 0%

commit v1 on v0

--- a/solution.py
+++ b/solution.py
@@ -119,7 +119,7 @@
     token_factor = (length * fs_count) ** (-0.5)
     rank_here = moments.shape[0]
     cols_here = moments.shape[2]
-    factor_wide = factors.astype(jnp.float32)
+    whole_weights = lax.all_gather(weights.astype(jnp.bfloat16), FS, axis=0, tiled=True)
     whole_factors = collect(factors, FS, 0)
     reduced = jnp.einsum("td,dkr->tkr", inputs, whole_factors, preferred_element_type=jnp.float32)
     reduced_upper = reduced.astype(jnp.bfloat16)
@@ -130,16 +130,25 @@
     lower_part = jnp.einsum(
         "tkr,tke->rke", reduced_lower, cotangents, preferred_element_type=jnp.float32
     )
-    projected = sum_at_owner(upper_part + lower_part, FS, 0)
-    projected = projected * token_factor
+    partial = ((upper_part + lower_part) * token_factor).astype(jnp.bfloat16)
+    parts = lax.all_to_all(in_blocks(partial, 0, fs_count), FS, 0, 0, tiled=True)
+    projected = jnp.sum(parts.astype(jnp.float32), axis=0)
     new_moments = BETA * moments + projected
-    local_sums = jnp.sum(new_moments * new_moments, axis=(0, 2))
-    totals = by_axis(local_sums, FS_TP)
+    whole_moments = collect(new_moments.astype(jnp.bfloat16), FS, 0)
+    wide_moments = whole_moments.astype(jnp.float32)
+    totals = lax.psum(jnp.sum(wide_moments * wide_moments, axis=(0, 2)), "tp")
     entries = rank_here * fs_count * cols_here * lax.axis_size("tp")
     rate = RATE_BASE / jnp.sqrt(1.0 + totals / entries)
-    low_part = jnp.einsum("dkr,rke->dke", factor_wide, collect(new_moments, FS, 0))
-    step = low_part * rate[None, :, None]
-    copies = lax.all_gather((weights - step).astype(jnp.bfloat16), FS, axis=0, tiled=True)
+    own_part = jnp.einsum(
+        "dkr,rke->dke", factors, whole_moments, preferred_element_type=jnp.float32
+    )
+    step = own_part * rate[None, :, None]
+    low_part = jnp.einsum(
+        "dkr,rke->dke", whole_factors, whole_moments, preferred_element_type=jnp.float32
+    )
+    copies = (whole_weights.astype(jnp.float32) - low_part * rate[None, :, None]).astype(
+        jnp.bfloat16
+    )
     return (step, new_moments, copies)
 
 

time: 264 us -> 182 us (0.69)
  waiting for transfers between devices: 97.7 us -> 28.3 us
  blocking collectives: 79.9 us -> 57.2 us
  local copies, waits for them, and re-layouts: 28.4 us -> 38.4 us
  matrix products: 14.2 us -> 20.5 us
  starting transfers between devices: 18 us -> 12.4 us
    all_gather x1, waiting for transfers between devices: 74.3 us -> 0.01 us  [per_device(): lax.all_gather(weights.astype(jnp.bfloat16), FS, axis=0, tiled=True)]
    psum x4 -> x1, blocking collectives: 45.8 us -> 10.9 us  [per_device(): totals = lax.psum(jnp.sum(wide_moments * wide_moments, axis=(0, 2)), 'tp')]
    all_to_all x1 -> x2, blocking collectives: 34.1 us -> 46.4 us  [the longest x1 23.9 us: sent_to_all(): return lax.all_to_all(copies, axis, split_axis=0, concat_axis=0, tiled=True)]
    all_gather x0 -> x1, local copies, waits for them, and re-layouts: none -> 11.1 us  [per_device(): lax.all_gather(weights.astype(jnp.bfloat16), FS, axis=0, tiled=True)]
    dot_general x1 -> x2, matrix products: 0.83 us -> 7.13 us  [the longest x1 6.97 us: per_device(): jnp.einsum('dkr,rke->dke', whole_factors, whole_moments, preferred_elemen...]
    all_to_all x2 -> x1, starting transfers between devices: 18 us -> 12.3 us  [sent_to_all(): return lax.all_to_all(copies, axis, split_axis=0, concat_axis=0, tiled=True)]
    all_to_all x2 -> x1, waiting for transfers between devices: 23.4 us -> 28.3 us  [sent_to_all(): return lax.all_to_all(copies, axis, split_axis=0, concat_axis=0, tiled=True)]
    unnamed x28 -> x26, local copies, waits for them, and re-layouts: 13.5 us -> 15.5 us
  transfers between devices with their start and end apart: 3 -> 2, of which waited for: 2 -> 1; matrix products, arithmetic and copies ran while one was open for 10% -> 19% of each run, Pallas kernels for 0% -> 0%
where the time goes in v1:
time: 182 us; the launch traced here: 181 us
  blocking collectives  57.2 us (31%)
  local copies, waits for them, and re-layouts  38.4 us (21%)
  waiting for transfers between devices  28.3 us (16%)
  matrix products  20.5 us (11%)
  between operations  14.3 us (8%)
  starting transfers between devices  12.4 us (7%)
  other arithmetic  6.89 us (4%)
  loops' own time  2.83 us (2%)
    all_to_all x1, waiting for transfers between devices, sent_to_all(): return lax.all_to_all(copies, axis, split_axis=0, concat_axis=0, tiled=True)  28.3 us
    all_to_all x1, blocking collectives, sent_to_all(): return lax.all_to_all(copies, axis, split_axis=0, concat_axis=0, tiled=True)  23.9 us
    all_to_all x1, blocking collectives, per_device(): lax.all_to_all(in_blocks(partial, 0, fs_count), FS, 0, 0, tiled=True)  22.5 us
    unnamed x26, local copies, waits for them, and re-layouts  15.5 us
    all_to_all x1, starting transfers between devices, sent_to_all(): return lax.all_to_all(copies, axis, split_axis=0, concat_axis=0, tiled=True)  12.3 us
    all_gather x1, local copies, waits for them, and re-layouts, per_device(): lax.all_gather(weights.astype(jnp.bfloat16), FS, axis=0, tiled=True)  11.1 us
    psum x1, blocking collectives, per_device(): totals = lax.psum(jnp.sum(wide_moments * wide_moments, axis=(0, 2)), 'tp')  10.9 us
    dot_general x1, matrix products, per_device(): jnp.einsum('dkr,rke->dke', whole_factors, whole_moments, preferred_elemen...  6.97 us
  transfers between devices with their start and end apart: 2, of which 1 were waited for; matrix products, arithmetic and copies ran while one was open for 19% of the time, Pallas kernels for 0%

profile of v1, /device:TPU:2, one launch (start us, length us, event | category | flops | bytes accessed | tf_op | source)
XLA Modules:
  0.0 180.9 jit_solution(321128160085733115)
XLA Ops:
  7.2 1.7 convert_element_type.69
  8.9 0.8 copy.74
  9.7 1.6 broadcast_in_dim.27
  11.3 12.3 %all-to-all-start = ((bf16[64,32,2,256]{3,1,2,0:T(8,128)(2,1)}), bf16[64,32,2,256]{3,1,2,0:T(8,128)(2,1)}, u32[]{:S(2)}, u32[]{:S(2)}) async-start(bf16[64,32,2,256]{3,1,2,0:T(8,128)(2,1)} %broadcast_in_dim.27), calls=%async_computation | async-start | bytes 4194304 | tf_op jit(solution)/shard_map/all_to_all | solution.py:18
  24.3 1.2 copy.69
  25.6 23.9 %while.12 = (s32[]{:T(128)}, bf16[4,384,128]{1,2,0:T(8,128)(2,1)}, bf16[4,384,128]{2,1,0:T(8,128)(2,1)}, bf16[4,384,2,64]{1,3,2,0:T(8,128)(2,1)S(1)}, bf16[4,384...) while((s32[]{:T(128)}, bf16[4,384,128]{1,2,0:T(8,128)(2,1)}, ...), condition=%wide.region_9.10_spmd, body=%wide.region_0.9_spmd.sunk | while | flops 195525504 | bytes 10978449 | solution.py:112
  25.6 0.6 dynamic_slice.47
  26.9 0.3 fusion.71
  27.3 0.3 fusion.69
  27.7 0.9 subtract_convert_fusion.4
  28.9 1.0 fusion.75
  29.9 0.4 multiply_reduce_fusion.7
  30.9 0.6 constant_dynamic-update-slice_fusion.2
  31.6 0.6 dynamic_slice.47
  33.3 0.3 fusion.69
  33.7 0.9 subtract_convert_fusion.4
  34.8 1.0 fusion.75
  35.8 0.4 multiply_reduce_fusion.7
  36.9 0.7 constant_dynamic-update-slice_fusion.2
  37.5 0.6 dynamic_slice.47
  39.2 0.3 fusion.69
  39.7 0.9 subtract_convert_fusion.4
  40.8 1.0 fusion.75
  41.8 0.4 multiply_reduce_fusion.7
  42.9 0.6 constant_dynamic-update-slice_fusion.2
  43.5 0.6 dynamic_slice.47
  45.2 0.3 fusion.69
  45.7 0.9 subtract_convert_fusion.4
  46.8 1.0 fusion.75
  47.8 0.4 multiply_reduce_fusion.7
  48.8 0.7 constant_dynamic-update-slice_fusion.2
  49.5 1.3 copy.73
  50.9 1.2 copy.91
  52.1 28.3 %all-to-all-done = bf16[64,32,2,256]{3,1,2,0:T(8,128)(2,1)} async-done(((bf16[64,32,2,256]{3,1,2,0:T(8,128)(2,1)}), bf16[64,32,2,256]{3,1,2,0:T(8,128)(2,1)}, u32[]{:S(2)}, u32[]{:S(2)}) %all-to-all-start) | async-done | bytes 2097184 | tf_op jit(solution)/shard_map/all_to_all | solution.py:18
  80.4 1.8 copy.75
  82.2 1.0 fusion.31
  83.2 0.3 copy-done.1
  83.5 0.5 fusion.37
  84.0 0.5 fusion.35
  84.9 22.5 %all_to_all.15 = bf16[64,4,2,512]{3,1,2,0:T(4,128)(2,1)S(1)} all-to-all(bf16[64,4,2,512]{3,1,2,0:T(4,128)(2,1)S(1)} %copy.78), channel_id=1, replica_groups=mesh['fs_0'=8,'fs_1'=4,'fs_2'=2,'tp'=4] {'fs_0','fs_1','fs_2'}, dimensions={0} | all-to-all | bytes 1048576 | tf_op jit(solution)/shard_map/all_to_all | solution.py:134
  107.7 23.9 %all_to_all.16 = bf16[64,4,2,512]{3,1,2,0:T(4,128)(2,1)S(1)} all-to-all(bf16[64,4,2,512]{3,1,2,0:T(4,128)(2,1)S(1)} %broadcast_in_dim.28), channel_id=1, replica_groups=mesh['fs_0'=8,'fs_1'=4,'fs_2'=2,'tp'=4] {'fs_0','fs_1','fs_2'}, dimensions={0} | all-to-all | bytes 1048576 | tf_op jit(solution)/shard_map/all_to_all | solution.py:18
  131.6 0.4 multiply_reduce_fusion.3
  132.0 0.6 copy.86
  132.6 10.9 %psum.7 = f32[2]{0:T(128)S(1)} all-reduce(f32[2]{0:T(128)S(1)} %multiply_reduce_fusion.3), channel_id=1, replica_groups=mesh['fs_0'=8,'fs_1'=4,'fs_2'=2,'tp'=4] {'tp'}, use_global_device_ids=true, to_apply=%region_12.13 | all-reduce | flops 2 | bytes 16 | tf_op jit(solution)/shard_map/psum | solution.py:139
  144.0 0.8 copy.85
  144.8 11.1 %copy.83 = bf16[2048,2,512]{0,2,1:T(8,128)(2,1)} copy(bf16[2048,2,512]{2,1,0:T(2,128)(2,1)} %all-gather.2.cloned.1.call-done) | data formatting | bytes 8388608 | tf_op jit(solution)/shard_map/all_gather | solution.py:122
  155.9 7.0 %fusion.30 = bf16[2048,2,512]{0,2,1:T(8,128)(2,1)} fusion(bf16[2048,2,512]{0,2,1:T(8,128)(2,1)} %copy.83, bf16[256,2,512]{2,0,1:T(8,128)(2,1)S(1)} %reshape.63, bf16[2048,2,256]{2,0,1:T(8,128)(2,1)} %bitcast.129, f32[2]{0:T(128)S(1)} %rsqrt_multiply_fusion), kind=kOutput, calls=%fused_computation.55 | convolution fusion | flops 1082130432 | bytes 11010056 | tf_op jit(solution)/shard_map/dkr,rke->dke/dot_general | solution.py:146
  162.9 11.1 %copy.87 = bf16[2048,2,512]{2,1,0:T(2,128)(2,1)} copy(bf16[2048,2,512]{0,2,1:T(8,128)(2,1)} %fusion.30) | data formatting | bytes 8388608
  (74 shorter events, 7.4 us)
Async XLA Ops:
  7.2 75.0 %copy-start = (bf16[384,2048]{1,0:T(8,128)(2,1)S(1)}, bf16[384,2048]{1,0:T(8,128)(2,1)}, u32[]{:S(2)}) copy-start(bf16[384,2048]{1,0:T(8,128)(2,1)} %param.12) | copy-start | bytes 4718596
  7.2 137.6 %all-gather.2.cloned.1.call-start = ((), (), s32[]{:S(2)}) async-start(), calls=%async_computation.3 | async-start | bytes 4259840 | tf_op jit(solution)/shard_map/all_gather | solution.py:122
  11.3 12.4 %copy-start.2 = (bf16[384,512]{1,0:T(8,128)(2,1)S(1)}, bf16[384,512]{1,0:T(8,128)(2,1)}, u32[]{:S(2)}) copy-start(bf16[384,512]{1,0:T(8,128)(2,1)} %param.13) | copy-start | bytes 1179652
  11.3 12.6 %copy-start.3 = (bf16[384,512]{1,0:T(8,128)(2,1)S(1)}, bf16[384,512]{1,0:T(8,128)(2,1)}, u32[]{:S(2)}) copy-start(bf16[384,512]{1,0:T(8,128)(2,1)} %param.14) | copy-start | bytes 1179652
  11.3 12.8 %copy-start.4 = (bf16[384,512]{1,0:T(8,128)(2,1)S(1)}, bf16[384,512]{1,0:T(8,128)(2,1)}, u32[]{:S(2)}) copy-start(bf16[384,512]{1,0:T(8,128)(2,1)} %param.15) | copy-start | bytes 1179652
  11.3 69.1 %all-to-all-start = ((bf16[64,32,2,256]{3,1,2,0:T(8,128)(2,1)}), bf16[64,32,2,256]{3,1,2,0:T(8,128)(2,1)}, u32[]{:S(2)}, u32[]{:S(2)}) async-start(bf16[64,32,2,256]{3,1,2,0:T(8,128)(2,1)} %broadcast_in_dim.27), calls=%async_computation | async-start | bytes 4194304 | tf_op jit(solution)/shard_map/all_to_all | solution.py:18
  23.6 1.9 %copy-start.6 = (f32[128]{0:T(128)S(1)}, f32[128]{0:T(128)}, u32[]{:S(2)}) copy-start(f32[128]{0:T(128)} %param.18) | copy-start | bytes 1540
  23.6 1.9 %copy-start.8 = (f32[4]{0:T(128)S(1)}, f32[4]{0:T(128)}, u32[]{:S(2)}) copy-start(f32[4]{0:T(128)} %param.17) | copy-start | bytes 52
  82.2 1.3 copy-start.1
  84.5 23.0 %copy-start.7 = (f32[4,2,512]{2,1,0:T(2,128)S(1)}, f32[4,2,512]{2,1,0:T(2,128)}, u32[]{:S(2)}) copy-start(f32[4,2,512]{2,1,0:T(2,128)} %param.20) | copy-start | bytes 49156
  107.6 36.3 %copy-start.5 = (bf16[32,2,256]{2,1,0:T(2,128)(2,1)S(1)}, bf16[32,2,256]{2,1,0:T(2,128)(2,1)}, u32[]{:S(2)}) copy-start(bf16[32,2,256]{2,1,0:T(2,128)(2,1)} %param.19) | copy-start | bytes 98308
Sparse Core Ops, SparseCore 0:
  10.8 87.8 all-gather.1

commit v2 on v0

v2 whole, which is shorter than its diff:
```python
import functools

import jax
import jax.numpy as jnp
from jax import lax
from jax.experimental import pallas as pl
from jax.experimental.pallas import tpu as pltpu
from jax.sharding import Mesh
from jax.sharding import PartitionSpec as P

PLANE = ("fs_0", "fs_1")
CORE = "fs_2"
FS = (*PLANE, CORE)

EPS = 0.05
BETA = 0.9
RATE_BASE = 0.5
BF16 = jnp.bfloat16
F32 = jnp.float32


def nt_dot(left, right):
    return lax.dot_general(left, right, (((1,), (1,)), ((), ())), preferred_element_type=F32)


def tn_dot(left, right):
    return lax.dot_general(left, right, (((0,), (0,)), ((), ())), preferred_element_type=F32)


def attention_kernel(rows, mix_ref, q_ref, k_ref, v_ref, up_ref, gain_ref, dq_ref, dv_ref, sum_ref):
    length, width = q_ref.shape
    head_dim = width // 2
    factor = head_dim**-0.5
    weight_mix = mix_ref[pl.program_id(0)]
    gain = gain_ref[...]
    for start in range(0, length, rows):
        seen = start + rows
        query = q_ref[start:seen, :]
        keys = k_ref[:seen, :]
        value = v_ref[:seen, :]
        place = lax.broadcasted_iota(jnp.int32, (rows, seen), 0) + start
        causal = lax.broadcasted_iota(jnp.int32, (rows, seen), 1) <= place

        def probs(which):
            cols = slice(which * head_dim, (which + 1) * head_dim)
            scores = nt_dot(query[:, cols], keys[:, cols]) * factor
            scores = jnp.where(causal, scores, -jnp.inf)
            expo = jnp.exp(scores - jnp.max(scores, axis=-1, keepdims=True))
            return expo * (1.0 / jnp.sum(expo, axis=-1, keepdims=True))

        first = probs(0)
        second = weight_mix * probs(1)
        mixed = (first - second).astype(BF16)
        output = jnp.dot(mixed, value, preferred_element_type=F32)
        inverse = lax.rsqrt(jnp.mean(output * output, axis=-1, keepdims=True) + EPS)
        scaled = gain * up_ref[start:seen, :].astype(F32)
        along = jnp.mean(output * scaled, axis=-1, keepdims=True)
        d_out = (inverse * scaled - output * (inverse * inverse * inverse * along)).astype(BF16)
        d_value = tn_dot(mixed, d_out)
        if start:
            sum_ref[:start, :] += d_value[:start]
        sum_ref[start:seen, :] = d_value[start:]
        d_mix = nt_dot(d_out, value)
        first_mix = jnp.sum(first * d_mix, axis=-1, keepdims=True)
        second_mix = jnp.sum(second * d_mix, axis=-1, keepdims=True) * (1.0 / weight_mix)
        d_first = (first * (d_mix - first_mix)).astype(BF16)
        d_second = (second * (second_mix - d_mix)).astype(BF16)
        dq_ref[start:seen, :head_dim] = (
            jnp.dot(d_first, keys[:, :head_dim], preferred_element_type=F32) * factor
        ).astype(BF16)
        dq_ref[start:seen, head_dim:] = (
            jnp.dot(d_second, keys[:, head_dim:], preferred_element_type=F32) * factor
        ).astype(BF16)
    dv_ref[...] = sum_ref[...].astype(BF16)


def attention_grads(queries, keys, values, head_cot, mixing, head_gain, rows=128):
    length, cols = queries.shape
    heads = mixing.shape[0]
    width = cols // heads
    block = pl.BlockSpec((length, width), lambda h: (0, h))
    return pl.pallas_call(
        functools.partial(attention_kernel, rows),
        grid=(heads,),
        in_specs=[
            pl.BlockSpec(memory_space=pltpu.SMEM),
            block,
            block,
            block,
            block,
            pl.BlockSpec((1, width), lambda h: (0, 0)),
        ],
        out_specs=[block, block],
        out_shape=[jax.ShapeDtypeStruct((length, cols), BF16)] * 2,
        scratch_shapes=[pltpu.VMEM((length, width), F32)],
        cost_estimate=pl.CostEstimate(
            flops=20 * length * length * cols,
            transcendentals=2 * heads * length * length,
            bytes_accessed=12 * length * cols,
        ),
        name="attention_grads",
    )(mixing, queries, keys, values, head_cot, head_gain.reshape(1, width))


def low_rank_rows(scale_ref, factor_rows, moment_ref, rows_ref):
    maps, rank, cols = moment_ref.shape
    count = factor_rows.shape[0]
    tiles = cols // 128
    for k in range(maps):
        part = jnp.dot(
            factor_rows[:, k * rank : (k + 1) * rank], moment_ref[k], preferred_element_type=F32
        )
        part = part * scale_ref[k]
        for j in range(tiles):
            rows_ref[pl.ds(maps * j + k, count, stride=maps * tiles), :] = part[
                :, j * 128 : (j + 1) * 128
            ]


def update_kernel(scale_ref, own_ref, factor_ref, moment_ref, weight_ref, step_ref, copy_ref, rows_ref):
    @pl.when(pl.program_id(0) == 0)
    def _():
        low_rank_rows(scale_ref, own_ref[...], moment_ref, step_ref)

    low_rank_rows(scale_ref, factor_ref[...], moment_ref, rows_ref)
    copy_ref[...] = (weight_ref[...].astype(F32) - rows_ref[...]).astype(BF16)


def update(rate, own_factors, whole_factors, whole_moments, whole_weights, rows=256):
    depth, width = whole_factors.shape
    own_depth = own_factors.shape[0]
    maps, rank, cols = whole_moments.shape
    each = maps * cols // 128
    return pl.pallas_call(
        update_kernel,
        grid=(depth // rows,),
        in_specs=[
            pl.BlockSpec(memory_space=pltpu.SMEM),
            pl.BlockSpec((own_depth, width), lambda i: (0, 0)),
            pl.BlockSpec((rows, width), lambda i: (i, 0)),
            pl.BlockSpec((maps, rank, cols), lambda i: (0, 0, 0)),
            pl.BlockSpec((rows * each, 128), lambda i: (i, 0)),
        ],
        out_specs=[
            pl.BlockSpec((own_depth * each, 128), lambda i: (0, 0)),
            pl.BlockSpec((rows * each, 128), lambda i: (i, 0)),
        ],
        out_shape=[
            jax.ShapeDtypeStruct((own_depth * each, 128), F32),
            jax.ShapeDtypeStruct((depth * each, 128), BF16),
        ],
        scratch_shapes=[pltpu.VMEM((rows * each, 128), F32)],
        cost_estimate=pl.CostEstimate(
            flops=2 * depth * maps * rank * cols,
            transcendentals=0,
            bytes_accessed=2 * depth * width + 4 * depth * maps * cols,
        ),
        name="low_rank_update",
    )(rate, own_factors, whole_factors, whole_moments, whole_weights)


def as_rows(array):
    depth, maps, cols = array.shape
    tiles = array.reshape(depth, maps, cols // 128, 128).transpose(0, 2, 1, 3)
    return tiles.reshape(depth * maps * cols // 128, 128)


def from_rows(rows, maps, cols):
    tiles = rows.reshape(-1, cols // 128, maps, 128).transpose(0, 2, 1, 3)
    return tiles.reshape(-1, maps, cols)


def sent_to_all(shard, axis):
    copies = jnp.broadcast_to(shard, (lax.axis_size(axis), *shard.shape))
    return lax.all_to_all(copies, axis, split_axis=0, concat_axis=0, tiled=True)


def gather_rows(shard, beside):
    mine, beside = lax.optimization_barrier((sent_to_all(shard, PLANE), beside))
    other = lax.ppermute(mine, CORE, [(0, 1), (1, 0)])
    low = lax.axis_index(CORE) == 0
    both = jnp.stack([jnp.where(low, mine, other), jnp.where(low, other, mine)], axis=1)
    return both.reshape(-1, *shard.shape[1:]), beside


def per_device(
    inputs, queries, keys, values, head_cot, mixing, head_gain, factors, moments, weights
):
    length = inputs.shape[0]
    fs_count = lax.axis_size(FS)
    token_factor = (length * fs_count) ** (-0.5)
    rank_here, maps, cols = moments.shape
    rank = rank_here * fs_count
    whole_weights = lax.all_gather(as_rows(weights).astype(BF16), FS, axis=0, tiled=True)
    own_factors = factors.reshape(-1, maps * rank)
    cotangents = attention_grads(queries, keys, values, head_cot, mixing, head_gain)
    whole_factors, cotangents = gather_rows(own_factors, cotangents)
    reduced = jnp.dot(inputs, whole_factors, preferred_element_type=F32)
    upper = reduced.astype(BF16)
    lower = (reduced - upper.astype(F32)).astype(BF16)
    partial = jnp.stack(
        [
            tn_dot(upper[:, k * rank : (k + 1) * rank], cotangents[k])
            + tn_dot(lower[:, k * rank : (k + 1) * rank], cotangents[k])
            for k in range(maps)
        ]
    )
    partial = (partial * token_factor).astype(BF16).reshape(maps, fs_count, rank_here, cols)
    partial = partial.transpose(1, 0, 2, 3).reshape(fs_count, maps * rank_here, cols)
    parts = lax.all_to_all(partial, FS, 0, 0, tiled=True)
    projected = jnp.sum(parts.astype(F32), axis=0).reshape(maps, rank_here, cols)
    new_moments = BETA * moments + projected.transpose(1, 0, 2)
    sent = new_moments.astype(BF16).transpose(1, 0, 2).reshape(maps * rank_here, cols)
    whole_moments = sent_to_all(sent, FS).reshape(fs_count, maps, rank_here, cols)
    whole_moments = whole_moments.transpose(1, 0, 2, 3).reshape(maps, rank, cols)
    wide = whole_moments.astype(F32)
    totals = lax.psum(jnp.sum(wide * wide, axis=(1, 2)), "tp")
    rate = RATE_BASE / jnp.sqrt(1.0 + totals / (rank * cols * lax.axis_size("tp")))
    step, copies = update(rate, own_factors, whole_factors, whole_moments, whole_weights)
    return (from_rows(step, maps, cols), new_moments, from_rows(copies, maps, cols))


def solution(mesh):
    torus = Mesh(mesh.devices.reshape(8, 4, 2, mesh.shape["tp"]), (*FS, "tp"))
    placed = (
        P(FS, None),
        P(FS, "tp"),
        P(FS, "tp"),
        P(FS, "tp"),
        P(FS, "tp"),
        P("tp"),
        P(),
        P(FS, None, None),
        P(FS, None, "tp"),
        P(FS, None, "tp"),
    )
    return jax.shard_map(
        per_device,
        mesh=torus,
        in_specs=placed,
        out_specs=(P(FS, None, "tp"), P(FS, None, "tp"), P(None, None, "tp")),
        check_vma=False,
    )
```

time: 264 us -> 145 us (0.55); the launches traced: 260 us -> 144 us
  waiting for transfers between devices: 97.7 us -> 20.2 us
  local copies, waits for them, and re-layouts: 28.4 us -> 5.34 us
  Pallas kernels: 0 us -> 21.6 us
  blocking collectives: 79.9 us -> 61.7 us
  matrix products: 14.2 us -> 5.07 us
  starting transfers between devices: 18 us -> 11.7 us
  loops' own time: 2.83 us -> 0 us
    all_gather x1, waiting for transfers between devices: 74.3 us -> 0.01 us  [per_device(): lax.all_gather(as_rows(weights).astype(BF16), FS, axis=0, tiled=True)]
    psum x4 -> x1, blocking collectives: 45.8 us -> 10.8 us  [per_device(): totals = lax.psum(jnp.sum(wide * wide, axis=(1, 2)), 'tp')]
    pallas_call x0 -> x2, Pallas kernels: none -> 21.6 us  [the longest x1 12.8 us: attention_grads(): pl.pallas_call(functools.partial(attention_kernel, rows), grid=(heads,),...]
    all_to_all x1 -> x2, blocking collectives: 34.1 us -> 50.9 us  [the longest x1 27.9 us: per_device(): parts = lax.all_to_all(partial, FS, 0, 0, tiled=True)]
    unnamed x28 -> x14, local copies, waits for them, and re-layouts: 13.5 us -> 1.76 us
    dot_general x32 -> x5, matrix products: 14.2 us -> 5.07 us  [the longest x4 3.03 us: tn_dot(): lax.dot_general(left, right, (((0,), (0,)), ((), ())), preferred_element_...]
    all_to_all x2 -> x1, starting transfers between devices: 18 us -> 11.6 us  [sent_to_all(): return lax.all_to_all(copies, axis, split_axis=0, concat_axis=0, tiled=True)]
    all_to_all x2 -> x1, waiting for transfers between devices: 23.4 us -> 17.4 us  [sent_to_all(): return lax.all_to_all(copies, axis, split_axis=0, concat_axis=0, tiled=True)]
  transfers between devices with their start and end apart: 3 -> 3, of which waited for: 2 -> 2; matrix products, arithmetic and copies ran while one was open for 10% -> 9% of each run, Pallas kernels for 0% -> 9%
where the time goes in v2:
time: 145 us; the launch traced here: 144 us
  blocking collectives  61.7 us (43%)
  Pallas kernels  21.6 us (15%)
  waiting for transfers between devices  20.2 us (14%)
  between operations  14.2 us (10%)
  starting transfers between devices  11.7 us (8%)
  local copies, waits for them, and re-layouts  5.34 us (4%)
  matrix products  5.07 us (3%)
  other arithmetic  4.3 us (3%)
    all_to_all x1, blocking collectives, per_device(): parts = lax.all_to_all(partial, FS, 0, 0, tiled=True)  27.9 us
    all_to_all x1, blocking collectives, sent_to_all(): return lax.all_to_all(copies, axis, split_axis=0, concat_axis=0, tiled=True)  23 us
    all_to_all x1, waiting for transfers between devices, sent_to_all(): return lax.all_to_all(copies, axis, split_axis=0, concat_axis=0, tiled=True)  17.4 us
    pallas_call x1, Pallas kernels, attention_grads(): pl.pallas_call(functools.partial(attention_kernel, rows), grid=(heads,),...  12.8 us
    all_to_all x1, starting transfers between devices, sent_to_all(): return lax.all_to_all(copies, axis, split_axis=0, concat_axis=0, tiled=True)  11.6 us
    psum x1, blocking collectives, per_device(): totals = lax.psum(jnp.sum(wide * wide, axis=(1, 2)), 'tp')  10.8 us
    pallas_call x1, Pallas kernels, update(): pl.pallas_call(update_kernel, grid=(depth // rows,), in_specs=[pl.BlockSp...  8.8 us
    dot_general x4, matrix products, tn_dot(): lax.dot_general(left, right, (((0,), (0,)), ((), ())), preferred_element_...  3.03 us
  transfers between devices with their start and end apart: 3, of which 2 were waited for; matrix products, arithmetic and copies ran while one was open for 9% of the time, Pallas kernels for 9%

profile of v2, /device:TPU:2, one launch (start us, length us, event | category | flops | bytes accessed | tf_op | source)
XLA Modules:
  0.0 144.0 jit_solution(3607878195190267187)
XLA Ops:
  7.2 0.0 copy-start
  7.2 0.0 all-gather.2.cloned.1.call-start
  7.2 1.7 %convert_element_type.42 = bf16[32,2,512]{2,1,0:T(2,128)(2,1)} convert(f32[32,2,512]{2,1,0:T(2,128)} %param.19) | non-fusion elementwise | flops 32768 | bytes 196608 | tf_op jit(solution)/shard_map/convert_element_type | solution.py:194
  8.9 0.0 all-gather.2.cloned.1.call-update
  8.9 0.8 copy.37
  9.7 0.0 copy-start.4
  9.7 1.1 broadcast_in_dim.6
  10.8 11.6 %all-to-all-start = ((bf16[32,32,512]{2,1,0:T(8,128)(2,1)}), bf16[32,32,512]{2,1,0:T(8,128)(2,1)S(1)}, u32[]{:S(2)}, u32[]{:S(2)}) async-start(bf16[32,32,512]{2,1,0:T(8,128)(2,1)} %broadcast_in_dim.6), calls=%async_computation | async-start | bytes 2097152 | tf_op jit(solution)/shard_map/all_to_all | solution.py:175
  22.4 12.8 %attention_grads.1 = (bf16[384,512]{1,0:T(8,128)(2,1)}, bf16[384,512]{1,0:T(8,128)(2,1)}) custom-call(f32[4]{0:T(128)} %mix_ref.1, bf16[384,512]{1,0:T(8,128)(2,1)} %q_ref.1, bf16[384,512]{1,0:T(8,128)(2,1)} %k_ref.1, bf16[384,512]{1,0:T(8,128)(2,1)} %v_ref.1, bf16[384,512]{1,0:T(8,128)(2,1)} %up_ref.1, f32[1,128]{1,0:T(1,128)} %bitcast.55), custom_call_target="tpu_custom_call" | custom-call | flops 1509949440 | bytes 2359296 | tf_op jit(solution)/shard_map/attention_grads/pallas_call | solution.py:82
  35.2 0.0 copy-done.4
  35.3 17.4 %all-to-all-done = bf16[32,32,512]{2,1,0:T(8,128)(2,1)S(1)} async-done(((bf16[32,32,512]{2,1,0:T(8,128)(2,1)}), bf16[32,32,512]{2,1,0:T(8,128)(2,1)S(1)}, u32[]{:S(2)}, u32[]{:S(2)}) %all-to-all-start) | async-done | bytes 1048608 | tf_op jit(solution)/shard_map/all_to_all | solution.py:175
  52.6 0.0 collective-permute-start
  52.6 2.8 %collective-permute-done = bf16[32,32,512]{2,1,0:T(8,128)(2,1)} collective-permute-done((bf16[32,32,512]{2,1,0:T(8,128)(2,1)S(1)}, bf16[32,32,512]{2,1,0:T(8,128)(2,1)}, u32[]{:S(2)}, u32[]{:S(2)}) %collective-permute-start) | collective-permute-done | bytes 1048608 | tf_op jit(solution)/shard_map/ppermute | solution.py:180
  55.4 1.4 select_bitcast_fusion.1
  56.8 0.2 pad_maximum_fusion
  57.0 0.0 copy-start.1
  57.0 0.0 copy-done
  57.0 0.0 copy-start.3
  57.0 2.0 %subtract_convert_fusion = (bf16[384,512]{0,1:T(8,128)(2,1)S(1)}, bf16[384,512]{0,1:T(8,128)(2,1)}) fusion(bf16[2048,512]{1,0:T(8,128)(2,1)S(1)} %bitcast.44, bf16[384,2048]{1,0:T(8,128)(2,1)S(1)} %copy-done), kind=kOutput, calls=%fused_computation.10 | convolution fusion | flops 806092800 | bytes 4456448 | tf_op jit(solution)/shard_map/dot_general | solution.py:198
  59.1 0.0 copy-done.1
  59.1 0.0 copy-done.3
  59.1 1.2 fusion.2
  60.3 0.0 copy-start.2
  60.3 0.3 convolution_add_fusion
  60.6 0.1 stack.22
  60.8 0.2 copy.29
  61.0 0.3 copy-done.2
  61.3 1.2 fusion.5
  62.5 0.3 convolution_add_fusion.1
  62.8 0.1 stack.21
  63.0 0.2 copy.28
  63.2 0.0 copy-start.5
  63.2 0.1 fusion
  63.3 0.3 copy.30
  63.6 27.9 %all_to_all.15 = bf16[64,8,512]{2,1,0:T(8,128)(2,1)S(1)} all-to-all(bf16[64,8,512]{2,1,0:T(8,128)(2,1)S(1)} %copy.30), channel_id=1, replica_groups=mesh['fs_0'=8,'fs_1'=4,'fs_2'=2,'tp'=4] {'fs_0','fs_1','fs_2'}, dimensions={0} | all-to-all | bytes 1048576 | tf_op jit(solution)/shard_map/all_to_all | solution.py:210
  91.5 0.1 convert_reduce_fusion
  91.6 0.0 copy-done.5
  91.7 23.0 %all_to_all.16 = bf16[64,8,512]{2,1,0:T(8,128)(2,1)S(1)} all-to-all(bf16[64,8,512]{2,1,0:T(8,128)(2,1)S(1)} %broadcast_in_dim.7), channel_id=1, replica_groups=mesh['fs_0'=8,'fs_1'=4,'fs_2'=2,'tp'=4] {'fs_0','fs_1','fs_2'}, dimensions={0} | all-to-all | bytes 1048576 | tf_op jit(solution)/shard_map/all_to_all | solution.py:175
  114.7 0.2 copy.31
  114.9 0.3 multiply_reduce_fusion
  115.1 0.6 copy.36
  115.8 10.8 %psum.7 = f32[2]{0:T(128)S(1)} all-reduce(f32[2]{0:T(128)S(1)} %multiply_reduce_fusion), channel_id=1, replica_groups=mesh['fs_0'=8,'fs_1'=4,'fs_2'=2,'tp'=4] {'tp'}, use_global_device_ids=true, to_apply=%region_2.3 | all-reduce | flops 2 | bytes 16 | tf_op jit(solution)/shard_map/psum | solution.py:217
  126.5 0.4 copy.32
  126.9 0.9 reshape.58.moment_ref
  127.8 0.6 rsqrt_multiply_fusion.scale_ref
  128.4 0.0 all-gather.2.cloned.1.call-done.weight_ref
  128.4 8.8 %low_rank_update.1 = (f32[256,128]{1,0:T(8,128)}, bf16[16384,128]{1,0:T(8,128)(2,1)}) custom-call(f32[2]{0:T(128)} %rsqrt_multiply_fusion.scale_ref, bf16[32,512]{1,0:T(8,128)(2,1)} %bitcast.50, bf16[2048,512]{1,0:T(8,128)(2,1)} %bitcast.45, bf16[2,256,512]{2,1,0:T(8,128)(2,1)} %reshape.58.moment_ref, bf16[16384,128]{1,0:T(8,128)(2,1)} %all-gather.2.cloned.1.call-done.weight_ref), custom_call_target="tpu_custom_call" | custom-call | flops 1073741824 | bytes 10485760 | tf_op jit(solution)/shard_map/low_rank_update/pallas_call | solution.py:134
  (4 shorter events, 0.1 us)
Async XLA Ops:
  7.2 49.9 %copy-start = (bf16[384,2048]{1,0:T(8,128)(2,1)S(1)}, bf16[384,2048]{1,0:T(8,128)(2,1)}, u32[]{:S(2)}) copy-start(bf16[384,2048]{1,0:T(8,128)(2,1)} %param.10) | copy-start | bytes 4718596
  7.2 121.2 %all-gather.2.cloned.1.call-start = ((), (), s32[]{:S(2)}) async-start(), calls=%async_computation.3 | async-start | bytes 4259840 | tf_op jit(solution)/shard_map/all_gather | solution.py:194
  9.7 25.5 %copy-start.4 = (bf16[4,8,2,256]{3,1,2,0:T(8,128)(2,1)}, bf16[4,8,2,256]{3,1,2,0:T(8,128)(2,1)S(1)}, u32[]{:S(2)}) copy-start(bf16[4,8,2,256]{3,1,2,0:T(8,128)(2,1)S(1)} %copy.37) | copy-start | bytes 98308
  10.8 41.8 %all-to-all-start = ((bf16[32,32,512]{2,1,0:T(8,128)(2,1)}), bf16[32,32,512]{2,1,0:T(8,128)(2,1)S(1)}, u32[]{:S(2)}, u32[]{:S(2)}) async-start(bf16[32,32,512]{2,1,0:T(8,128)(2,1)} %broadcast_in_dim.6), calls=%async_computation | async-start | bytes 2097152 | tf_op jit(solution)/shard_map/all_to_all | solution.py:175
  52.6 2.8 %collective-permute-start = (bf16[32,32,512]{2,1,0:T(8,128)(2,1)S(1)}, bf16[32,32,512]{2,1,0:T(8,128)(2,1)}, u32[]{:S(2)}, u32[]{:S(2)}) collective-permute-start(bf16[32,32,512]{2,1,0:T(8,128)(2,1)S(1)} %all-to-all-done), channel_id=1, source_target_pairs={{0,4},{4,0},{1,5},{5,1},{2,6},{6,2},{3,7},{7,3},{8,12},{12,8},{9,1... | collective-permute-start | bytes 3145736 | tf_op jit(solution)/shard_map/ppermute | solution.py:180
  57.0 2.1 %copy-start.1 = (bf16[32,2,32,512]{3,2,1,0:T(8,128)(2,1)}, bf16[32,2,32,512]{3,2,1,0:T(8,128)(2,1)S(1)}, u32[]{:S(2)}) copy-start(bf16[32,2,32,512]{3,2,1,0:T(8,128)(2,1)S(1)} %pad_maximum_fusion) | copy-start | bytes 6291460
  57.0 2.1 %copy-start.3 = (bf16[384,512]{1,0:T(8,128)(2,1)S(1)}, bf16[384,512]{1,0:T(8,128)(2,1)}, u32[]{:S(2)}) copy-start(bf16[384,512]{1,0:T(8,128)(2,1)} %get-tuple-element.14) | copy-start | bytes 1179652
  60.3 1.0 copy-start.2
  63.2 28.5 %copy-start.5 = (f32[4,2,512]{2,1,0:T(2,128)S(1)}, f32[4,2,512]{2,1,0:T(2,128)}, u32[]{:S(2)}) copy-start(f32[4,2,512]{2,1,0:T(2,128)} %param.18) | copy-start | bytes 49156
Sparse Core Ops, SparseCore 0:
  11.3 87.1 all-gather.1

commit v3 on v2

--- a/solution.py
+++ b/solution.py
@@ -8,9 +8,10 @@
 from jax.sharding import Mesh
 from jax.sharding import PartitionSpec as P
 
-PLANE = ("fs_0", "fs_1")
-CORE = "fs_2"
+DEEP, WIDE, CORE = "fs_0", "fs_1", "fs_2"
+PLANE = (DEEP, WIDE)
 FS = (*PLANE, CORE)
+SWAP = [(0, 1), (1, 0)]
 
 EPS = 0.05
 BETA = 0.9
@@ -102,6 +103,96 @@
     )(mixing, queries, keys, values, head_cot, head_gain.reshape(1, width))
 
 
+def interleaved(first, second):
+    half = lax.broadcasted_iota(jnp.int32, first.shape, 0) % 8 < 4
+    count = first.shape[0]
+    even = jnp.where(half, first, pltpu.roll(second, 4, 0))
+    odd = jnp.where(half, pltpu.roll(first, count - 4, 0), second)
+    return even, odd
+
+
+def separated(even, odd):
+    half = lax.broadcasted_iota(jnp.int32, even.shape, 0) % 8 < 4
+    count = even.shape[0]
+    first = jnp.where(half, even, pltpu.roll(odd, 4, 0))
+    second = jnp.where(half, pltpu.roll(even, count - 4, 0), odd)
+    return first, second
+
+
+def fill_rows(low, mine_ref, other_ref, rows_ref):
+    xs, zs, rows, _ = mine_ref.shape
+    for z in range(zs):
+        for x in range(xs):
+            mine, other = mine_ref[x, z], other_ref[x, z]
+            at = 2 * rows * (z * xs + x)
+            rows_ref[at : at + rows, :] = jnp.where(low, mine, other)
+            rows_ref[at + rows : at + 2 * rows, :] = jnp.where(low, other, mine)
+
+
+def project_kernel(
+    scale, core_ref, mine_ref, other_ref, in_ref, dq_ref, dv_ref, keep_ref, send_ref, rows_ref, red_ref
+):
+    step = pl.program_id(0)
+    low = core_ref[0] == 0
+    fill_rows(low, mine_ref, other_ref, rows_ref)
+    part = jnp.dot(in_ref[...], rows_ref[...], preferred_element_type=F32)
+
+    @pl.when(step == 0)
+    def _():
+        red_ref[...] = part
+
+    @pl.when(step > 0)
+    def _():
+        red_ref[...] += part
+
+    @pl.when(step == pl.num_programs(0) - 1)
+    def _():
+        reduced = red_ref[...]
+        upper = reduced.astype(BF16)
+        lower = (reduced - upper.astype(F32)).astype(BF16)
+        rank = keep_ref.shape[0]
+        sums = []
+        for k, cot_ref in enumerate((dq_ref, dv_ref)):
+            cols = slice(k * rank, (k + 1) * rank)
+            cot = cot_ref[...]
+            sums.append((tn_dot(upper[:, cols], cot) + tn_dot(lower[:, cols], cot)) * scale)
+        even, odd = interleaved(*sums)
+        keep_ref[...] = jnp.where(low, even, odd)
+        send_ref[...] = jnp.where(low, odd, even)
+
+
+def project(scale, core, mine, other, inputs, d_query, d_value, each=2):
+    xs, zs, rows, width = mine.shape
+    length, depth = inputs.shape
+    cols = d_query.shape[1]
+    rank = width // 2
+    block = pl.BlockSpec((xs, each, rows, width), lambda i: (0, i, 0, 0))
+    span = 2 * xs * each * rows
+    whole = pl.BlockSpec((length, cols), lambda i: (0, 0))
+    result = pl.BlockSpec((rank, cols), lambda i: (0, 0))
+    return pl.pallas_call(
+        functools.partial(project_kernel, scale),
+        grid=(zs // each,),
+        in_specs=[
+            pl.BlockSpec(memory_space=pltpu.SMEM),
+            block,
+            block,
+            pl.BlockSpec((length, span), lambda i: (0, i)),
+            whole,
+            whole,
+        ],
+        out_specs=[result, result],
+        out_shape=[jax.ShapeDtypeStruct((rank, cols), F32)] * 2,
+        scratch_shapes=[pltpu.VMEM((span, width), BF16), pltpu.VMEM((length, width), F32)],
+        cost_estimate=pl.CostEstimate(
+            flops=2 * length * width * (depth + 2 * cols),
+            transcendentals=0,
+            bytes_accessed=2 * depth * (length + width) + 4 * length * cols + 8 * rank * cols,
+        ),
+        name="project",
+    )(core, mine, other, inputs, d_query, d_value)
+
+
 def low_rank_rows(scale_ref, factor_rows, moment_ref, rows_ref):
     maps, rank, cols = moment_ref.shape
     count = factor_rows.shape[0]
@@ -117,46 +208,80 @@
             ]
 
 
-def update_kernel(scale_ref, own_ref, factor_ref, moment_ref, weight_ref, step_ref, copy_ref, rows_ref):
+def update_kernel(
+    core_ref,
+    scale_ref,
+    own_ref,
+    mine_ref,
+    other_ref,
+    moment_mine_ref,
+    moment_other_ref,
+    weight_ref,
+    step_ref,
+    copy_ref,
+    factor_ref,
+    moment_ref,
+    rows_ref,
+):
+    low = core_ref[0] == 0
+
     @pl.when(pl.program_id(0) == 0)
     def _():
+        mine = moment_mine_ref[...].astype(F32)
+        other = moment_other_ref[...].astype(F32)
+        first, second = separated(jnp.where(low, mine, other), jnp.where(low, other, mine))
+        moment_ref[0] = first.astype(BF16)
+        moment_ref[1] = second.astype(BF16)
         low_rank_rows(scale_ref, own_ref[...], moment_ref, step_ref)
 
+    fill_rows(low, mine_ref, other_ref, factor_ref)
     low_rank_rows(scale_ref, factor_ref[...], moment_ref, rows_ref)
     copy_ref[...] = (weight_ref[...].astype(F32) - rows_ref[...]).astype(BF16)
 
 
-def update(rate, own_factors, whole_factors, whole_moments, whole_weights, rows=256):
-    depth, width = whole_factors.shape
+def update(core, rate, own_factors, mine, other, moments_mine, moments_other, whole_weights):
+    xs, zs, rows, width = mine.shape
+    rank, cols = moments_mine.shape
+    maps = width // rank
+    each = maps * cols // 128
+    span = 2 * xs * rows
+    depth = span * zs
     own_depth = own_factors.shape[0]
-    maps, rank, cols = whole_moments.shape
-    each = maps * cols // 128
+    block = pl.BlockSpec((xs, 1, rows, width), lambda i: (0, i, 0, 0))
+    moment_block = pl.BlockSpec((rank, cols), lambda i: (0, 0))
     return pl.pallas_call(
         update_kernel,
-        grid=(depth // rows,),
+        grid=(zs,),
         in_specs=[
             pl.BlockSpec(memory_space=pltpu.SMEM),
+            pl.BlockSpec(memory_space=pltpu.SMEM),
             pl.BlockSpec((own_depth, width), lambda i: (0, 0)),
-            pl.BlockSpec((rows, width), lambda i: (i, 0)),
-            pl.BlockSpec((maps, rank, cols), lambda i: (0, 0, 0)),
-            pl.BlockSpec((rows * each, 128), lambda i: (i, 0)),
+            block,
+            block,
+            moment_block,
+            moment_block,
+            pl.BlockSpec((span * each, 128), lambda i: (i, 0)),
         ],
         out_specs=[
             pl.BlockSpec((own_depth * each, 128), lambda i: (0, 0)),
-            pl.BlockSpec((rows * each, 128), lambda i: (i, 0)),
+            pl.BlockSpec((span * each, 128), lambda i: (i, 0)),
         ],
         out_shape=[
             jax.ShapeDtypeStruct((own_depth * each, 128), F32),
             jax.ShapeDtypeStruct((depth * each, 128), BF16),
         ],
-        scratch_shapes=[pltpu.VMEM((rows * each, 128), F32)],
+        scratch_shapes=[
+            pltpu.VMEM((span, width), BF16),
+            pltpu.VMEM((maps, rank, cols), BF16),
+            pltpu.VMEM((span * each, 128), F32),
+        ],
         cost_estimate=pl.CostEstimate(
-            flops=2 * depth * maps * rank * cols,
+            flops=2 * depth * width * cols,
             transcendentals=0,
             bytes_accessed=2 * depth * width + 4 * depth * maps * cols,
         ),
         name="low_rank_update",
-    )(rate, own_factors, whole_factors, whole_moments, whole_weights)
+    )(core, rate, own_factors, mine, other, moments_mine, moments_other, whole_weights)
 
 
 def as_rows(array):
@@ -175,48 +300,47 @@
     return lax.all_to_all(copies, axis, split_axis=0, concat_axis=0, tiled=True)
 
 
-def gather_rows(shard, beside):
-    mine, beside = lax.optimization_barrier((sent_to_all(shard, PLANE), beside))
-    other = lax.ppermute(mine, CORE, [(0, 1), (1, 0)])
-    low = lax.axis_index(CORE) == 0
-    both = jnp.stack([jnp.where(low, mine, other), jnp.where(low, other, mine)], axis=1)
-    return both.reshape(-1, *shard.shape[1:]), beside
-
-
 def per_device(
     inputs, queries, keys, values, head_cot, mixing, head_gain, factors, moments, weights
 ):
     length = inputs.shape[0]
+    planes = lax.axis_size(PLANE)
     fs_count = lax.axis_size(FS)
     token_factor = (length * fs_count) ** (-0.5)
     rank_here, maps, cols = moments.shape
     rank = rank_here * fs_count
+    core = lax.axis_index(CORE).reshape(1)
+    own_factors = factors.reshape(-1, maps * rank)
+    columns = sent_to_all(own_factors, DEEP)
+    columns, weights = lax.optimization_barrier((columns, weights))
     whole_weights = lax.all_gather(as_rows(weights).astype(BF16), FS, axis=0, tiled=True)
-    own_factors = factors.reshape(-1, maps * rank)
-    cotangents = attention_grads(queries, keys, values, head_cot, mixing, head_gain)
-    whole_factors, cotangents = gather_rows(own_factors, cotangents)
-    reduced = jnp.dot(inputs, whole_factors, preferred_element_type=F32)
-    upper = reduced.astype(BF16)
-    lower = (reduced - upper.astype(F32)).astype(BF16)
-    partial = jnp.stack(
-        [
-            tn_dot(upper[:, k * rank : (k + 1) * rank], cotangents[k])
-            + tn_dot(lower[:, k * rank : (k + 1) * rank], cotangents[k])
-            for k in range(maps)
-        ]
-    )
-    partial = (partial * token_factor).astype(BF16).reshape(maps, fs_count, rank_here, cols)
-    partial = partial.transpose(1, 0, 2, 3).reshape(fs_count, maps * rank_here, cols)
-    parts = lax.all_to_all(partial, FS, 0, 0, tiled=True)
+    mine = sent_to_all(columns, WIDE)
+    d_query, d_value = attention_grads(queries, keys, values, head_cot, mixing, head_gain)
+    mine, d_query, d_value = lax.optimization_barrier((mine, d_query, d_value))
+    other = lax.ppermute(mine, CORE, SWAP)
+    keep, send = project(token_factor, core, mine, other, inputs, d_query, d_value)
+    summed = (keep + lax.ppermute(send, CORE, SWAP)).astype(BF16)
+    summed = summed.reshape(planes, maps * rank_here, cols)
+    parts = lax.all_to_all(summed, PLANE, 0, 0, tiled=True)
     projected = jnp.sum(parts.astype(F32), axis=0).reshape(maps, rank_here, cols)
     new_moments = BETA * moments + projected.transpose(1, 0, 2)
     sent = new_moments.astype(BF16).transpose(1, 0, 2).reshape(maps * rank_here, cols)
-    whole_moments = sent_to_all(sent, FS).reshape(fs_count, maps, rank_here, cols)
-    whole_moments = whole_moments.transpose(1, 0, 2, 3).reshape(maps, rank, cols)
-    wide = whole_moments.astype(F32)
-    totals = lax.psum(jnp.sum(wide * wide, axis=(1, 2)), "tp")
+    moments_mine = sent_to_all(sent, PLANE)
+    moments_other = lax.ppermute(moments_mine, CORE, SWAP)
+    squares = moments_mine.astype(F32) ** 2 + moments_other.astype(F32) ** 2
+    squares = jnp.sum(squares.reshape(planes, maps, rank_here, cols), axis=(0, 2, 3))
+    totals = lax.psum(squares, "tp")
     rate = RATE_BASE / jnp.sqrt(1.0 + totals / (rank * cols * lax.axis_size("tp")))
-    step, copies = update(rate, own_factors, whole_factors, whole_moments, whole_weights)
+    step, copies = update(
+        core,
+        rate,
+        own_factors,
+        mine,
+        other,
+        moments_mine.reshape(rank, cols),
+        moments_other.reshape(rank, cols),
+        whole_weights,
+    )
     return (from_rows(step, maps, cols), new_moments, from_rows(copies, maps, cols))
 
 

time: 145 us -> 127 us (0.88)
  waiting for transfers between devices: 20.2 us -> 6.22 us
  starting transfers between devices: 11.7 us -> 5.1 us
  Pallas kernels: 21.6 us -> 27.6 us
  matrix products: 5.07 us -> 0 us
  blocking collectives: 61.7 us -> 65.2 us
  local copies, waits for them, and re-layouts: 5.34 us -> 3.64 us
    all_to_all x1, waiting for transfers between devices: 17.4 us -> 0.01 us  [sent_to_all(): return lax.all_to_all(copies, axis, split_axis=0, concat_axis=0, tiled=True)]
    all_to_all x1 -> x2, blocking collectives: 23 us -> 38.7 us  [sent_to_all(): return lax.all_to_all(copies, axis, split_axis=0, concat_axis=0, tiled=True)]
    all_to_all x1, blocking collectives: 27.9 us -> 16.3 us  [per_device(): parts = lax.all_to_all(summed, PLANE, 0, 0, tiled=True)]
    all_to_all x1, starting transfers between devices: 11.6 us -> 4.82 us  [sent_to_all(): return lax.all_to_all(copies, axis, split_axis=0, concat_axis=0, tiled=True)]
    pallas_call x1 -> x2, Pallas kernels: 8.8 us -> 14.8 us  [the longest x1 8.95 us: update(): pl.pallas_call(update_kernel, grid=(zs,), in_specs=[pl.BlockSpec(memory_s...]
    dot_general x5 -> x0, matrix products: 5.07 us -> none  [the longest x4 3.03 us: tn_dot(): lax.dot_general(left, right, (((0,), (0,)), ((), ())), preferred_element_...]
    ppermute x1 -> x3, waiting for transfers between devices: 2.79 us -> 6.2 us  [the longest x1 2.64 us: per_device(): other = lax.ppermute(mine, CORE, SWAP)]
    another operation x2 -> x0, other arithmetic: 1.57 us -> none  [gather_rows(): jnp.stack([jnp.where(low, mine, other), jnp.where(low, other, mine)], axi...]
  transfers between devices with their start and end apart: 3 -> 5, of which waited for: 2 -> 3; matrix products, arithmetic and copies ran while one was open for 9% -> 3% of each run, Pallas kernels for 9% -> 15%
where the time goes in v3:
time: 127 us; the launch traced here: 126 us
  blocking collectives  65.2 us (51%)
  Pallas kernels  27.6 us (22%)
  between operations  14.1 us (11%)
  waiting for transfers between devices  6.22 us (5%)
  starting transfers between devices  5.1 us (4%)
  other arithmetic  3.68 us (3%)
  local copies, waits for them, and re-layouts  3.64 us (3%)
    all_to_all x2, blocking collectives, sent_to_all(): return lax.all_to_all(copies, axis, split_axis=0, concat_axis=0, tiled=True)  38.7 us
    all_to_all x1, blocking collectives, per_device(): parts = lax.all_to_all(summed, PLANE, 0, 0, tiled=True)  16.3 us
    pallas_call x1, Pallas kernels, attention_grads(): pl.pallas_call(functools.partial(attention_kernel, rows), grid=(heads,),...  12.8 us
    psum x1, blocking collectives, per_device(): totals = lax.psum(squares, 'tp')  10.3 us
    pallas_call x1, Pallas kernels, update(): pl.pallas_call(update_kernel, grid=(zs,), in_specs=[pl.BlockSpec(memory_s...  8.95 us
    pallas_call x1, Pallas kernels, project(): pl.pallas_call(functools.partial(project_kernel, scale), grid=(zs // each...  5.82 us
    all_to_all x1, starting transfers between devices, sent_to_all(): return lax.all_to_all(copies, axis, split_axis=0, concat_axis=0, tiled=True)  4.82 us
    ppermute x1, waiting for transfers between devices, per_device(): other = lax.ppermute(mine, CORE, SWAP)  2.64 us
  transfers between devices with their start and end apart: 5, of which 3 were waited for; matrix products, arithmetic and copies ran while one was open for 3% of the time, Pallas kernels for 15%

profile of v3, /device:TPU:2, one launch (start us, length us, event | category | flops | bytes accessed | tf_op | source)
XLA Modules:
  0.0 125.6 jit_solution(17484794860168468946)
XLA Ops:
  7.2 0.0 all-gather.2.cloned.1.call-start
  7.2 0.8 copy.21
  8.0 0.0 copy-start.4
  8.0 20.1 %all_to_all.20 = bf16[8,32,512]{2,1,0:T(8,128)(2,1)S(1)} all-to-all(bf16[8,32,512]{2,1,0:T(8,128)(2,1)S(1)} %broadcast_in_dim.9), channel_id=1, replica_groups=mesh['fs_0'=8,'fs_1'=4,'fs_2'=2,'tp'=4] {'fs_0'}, dimensions={0} | all-to-all | bytes 524288 | tf_op jit(solution)/shard_map/all_to_all | solution.py:300
  28.1 1.6 %convert_element_type.32 = bf16[32,2,512]{2,1,0:T(2,128)(2,1)} convert(f32[32,2,512]{2,1,0:T(2,128)} %param.19) | non-fusion elementwise | flops 32768 | bytes 196608 | tf_op jit(solution)/shard_map/convert_element_type | solution.py:316
  29.7 0.0 all-gather.2.cloned.1.call-update
  29.7 1.1 broadcast_in_dim.10
  30.8 4.8 %all-to-all-start.1 = ((bf16[4,8,32,512]{3,2,1,0:T(8,128)(2,1)}), bf16[4,8,32,512]{3,2,1,0:T(8,128)(2,1)S(1)}, u32[]{:S(2)}, u32[]{:S(2)}) async-start(bf16[4,8,32,512]{3,2,1,0:T(8,128)(2,1)} %broadcast_in_dim.10), calls=%async_computation.1 | async-start | bytes 2097152 | tf_op jit(solution)/shard_map/all_to_all | solution.py:300
  35.7 12.8 %attention_grads.1 = (bf16[384,512]{1,0:T(8,128)(2,1)}, bf16[384,512]{1,0:T(8,128)(2,1)}) custom-call(f32[4]{0:T(128)} %mix_ref.1, bf16[384,512]{1,0:T(8,128)(2,1)} %q_ref.1, bf16[384,512]{1,0:T(8,128)(2,1)} %k_ref.1, bf16[384,512]{1,0:T(8,128)(2,1)} %v_ref.1, bf16[384,512]{1,0:T(8,128)(2,1)} %up_ref.1, f32[1,128]{1,0:T(1,128)} %bitcast.36), custom_call_target="tpu_custom_call" | custom-call | flops 1509949440 | bytes 2359296 | tf_op jit(solution)/shard_map/attention_grads/pallas_call | solution.py:83
  48.5 0.0 copy-done.4
  48.5 0.0 copy-start.5
  48.5 0.0 all-to-all-done.1.mine_ref
  48.5 0.0 copy-start
  48.5 0.1 collective-permute-start
  48.6 2.6 %collective-permute-done.other_ref = bf16[4,8,32,512]{3,2,1,0:T(8,128)(2,1)S(1)} collective-permute-done((bf16[4,8,32,512]{3,2,1,0:T(8,128)(2,1)S(1)}, bf16[4,8,32,512]{3,2,1,0:T(8,128)(2,1)S(1)}, u32[]{:S(2)}, u32[]{:S(2)}) %collective-permute-start) | collective-permute-done | bytes 1048608 | tf_op jit(solution)/shard_map/ppermute | solution.py:320
  51.3 0.0 copy-start.3
  51.3 0.0 copy-done
  51.3 1.0 copy-done.3
  52.3 5.8 %project.1 = (f32[256,512]{1,0:T(8,128)}, f32[256,512]{1,0:T(8,128)}) custom-call(s32[1]{0:T(128)} %bitcast.core_ref, bf16[4,8,32,512]{3,2,1,0:T(8,128)(2,1)} %copy-done, bf16[4,8,32,512]{3,2,1,0:T(8,128)(2,1)} %copy-done.3, bf16[384,2048]{1,0:T(8,128)(2,1)} %in_ref.1, bf16[384,512]{1,0:T(8,128)(2,1)} %get-tuple-element.18.dq_ref, ...), custom_call_target="tpu_custom_call" | custom-call | flops 1207959552 | bytes 5505024 | tf_op jit(solution)/shard_map/project/pallas_call | solution.py:173
  58.1 0.1 collective-permute-start.1
  58.2 2.0 %collective-permute-done.1 = f32[256,512]{1,0:T(8,128)S(1)} collective-permute-done((f32[256,512]{1,0:T(8,128)}, f32[256,512]{1,0:T(8,128)S(1)}, u32[]{:S(2)}, u32[]{:S(2)}) %collective-permute-start.1) | collective-permute-done | bytes 524320 | tf_op jit(solution)/shard_map/ppermute | solution.py:322
  60.2 1.1 fusion
  61.3 16.3 %all_to_all.21 = bf16[32,8,512]{2,1,0:T(8,128)(2,1)S(1)} all-to-all(bf16[32,8,512]{2,1,0:T(8,128)(2,1)S(1)} %fusion), channel_id=1, replica_groups=mesh['fs_0'=8,'fs_1'=4,'fs_2'=2,'tp'=4] {'fs_0','fs_1'}, dimensions={0} | all-to-all | bytes 524288 | tf_op jit(solution)/shard_map/all_to_all | solution.py:324
  77.7 0.0 copy-done.5
  77.8 18.5 %all_to_all.22 = bf16[32,8,512]{2,1,0:T(8,128)(2,1)S(1)} all-to-all(bf16[32,8,512]{2,1,0:T(8,128)(2,1)S(1)} %broadcast_in_dim.11), channel_id=1, replica_groups=mesh['fs_0'=8,'fs_1'=4,'fs_2'=2,'tp'=4] {'fs_0','fs_1'}, dimensions={0} | all-to-all | bytes 524288 | tf_op jit(solution)/shard_map/all_to_all | solution.py:300
  96.3 0.0 copy-start.1
  96.3 0.0 collective-permute-start.2
  96.3 1.6 %collective-permute-done.2 = bf16[32,8,512]{2,1,0:T(8,128)(2,1)S(1)} collective-permute-done((bf16[32,8,512]{2,1,0:T(8,128)(2,1)S(1)}, bf16[32,8,512]{2,1,0:T(8,128)(2,1)S(1)}, u32[]{:S(2)}, u32[]{:S(2)}) %collective-permute-start.2) | collective-permute-done | bytes 262176 | tf_op jit(solution)/shard_map/ppermute | solution.py:329
  97.9 0.0 copy-start.2
  97.9 0.2 add_reduce_fusion
  98.1 0.1 reduce_sum.27
  98.2 0.1 reduce_sum.28
  98.4 0.6 copy.20
  99.0 10.3 %psum.7 = f32[2]{0:T(128)S(1)} all-reduce(f32[2]{0:T(128)S(1)} %reduce_sum.28), channel_id=1, replica_groups=mesh['fs_0'=8,'fs_1'=4,'fs_2'=2,'tp'=4] {'tp'}, use_global_device_ids=true, to_apply=%region_3.4 | all-reduce | flops 2 | bytes 16 | tf_op jit(solution)/shard_map/psum | solution.py:332
  109.2 0.6 rsqrt_multiply_fusion.scale_ref
  109.8 0.0 all-gather.2.cloned.1.call-done.weight_ref
  109.8 0.0 copy-done.1
  109.8 0.0 copy-done.2
  109.8 9.0 %low_rank_update.1 = (f32[256,128]{1,0:T(8,128)}, bf16[16384,128]{1,0:T(8,128)(2,1)}) custom-call(s32[1]{0:T(128)} %bitcast.core_ref, f32[2]{0:T(128)} %rsqrt_multiply_fusion.scale_ref, bf16[32,512]{1,0:T(8,128)(2,1)} %bitcast.31, bf16[4,8,32,512]{3,2,1,0:T(8,128)(2,1)} %copy-done, bf16[4,8,32,512]{3,2,1,0:T(8,128)(2,1)} %copy-done.3, ...), custom_call_target="tpu_custom_call" | custom-call | flops 1073741824 | bytes 10485760 | tf_op jit(solution)/shard_map/low_rank_update/pallas_call | solution.py:252
  (6 shorter events, 0.1 us)
Async XLA Ops:
  7.2 102.6 %all-gather.2.cloned.1.call-start = ((), (), s32[]{:S(2)}) async-start(), calls=%async_computation.4 | async-start | bytes 4259840 | tf_op jit(solution)/shard_map/all_gather | solution.py:316
  8.0 40.5 %copy-start.4 = (bf16[4,8,2,256]{3,1,2,0:T(8,128)(2,1)}, bf16[4,8,2,256]{3,1,2,0:T(8,128)(2,1)S(1)}, u32[]{:S(2)}) copy-start(bf16[4,8,2,256]{3,1,2,0:T(8,128)(2,1)S(1)} %copy.21) | copy-start | bytes 98308
  30.8 17.7 %all-to-all-start.1 = ((bf16[4,8,32,512]{3,2,1,0:T(8,128)(2,1)}), bf16[4,8,32,512]{3,2,1,0:T(8,128)(2,1)S(1)}, u32[]{:S(2)}, u32[]{:S(2)}) async-start(bf16[4,8,32,512]{3,2,1,0:T(8,128)(2,1)} %broadcast_in_dim.10), calls=%async_computation.1 | async-start | bytes 2097152 | tf_op jit(solution)/shard_map/all_to_all | solution.py:300
  48.5 29.2 %copy-start.5 = (f32[4,2,512]{2,1,0:T(2,128)S(1)}, f32[4,2,512]{2,1,0:T(2,128)}, u32[]{:S(2)}) copy-start(f32[4,2,512]{2,1,0:T(2,128)} %param.18) | copy-start | bytes 49156
  48.5 2.8 %copy-start = (bf16[4,8,32,512]{3,2,1,0:T(8,128)(2,1)}, bf16[4,8,32,512]{3,2,1,0:T(8,128)(2,1)S(1)}, u32[]{:S(2)}) copy-start(bf16[4,8,32,512]{3,2,1,0:T(8,128)(2,1)S(1)} %all-to-all-done.1.mine_ref) | copy-start | bytes 3145732
  48.5 2.7 %collective-permute-start = (bf16[4,8,32,512]{3,2,1,0:T(8,128)(2,1)S(1)}, bf16[4,8,32,512]{3,2,1,0:T(8,128)(2,1)S(1)}, u32[]{:S(2)}, u32[]{:S(2)}) collective-permute-start(bf16[4,8,32,512]{3,2,1,0:T(8,128)(2,1)S(1)} %all-to-all-done.1.mine_ref), channel_id=1, source_target_pairs={{0,4},{4,0},{1,5},{5,1},{2,6},{6,2},{3,7},{7,3},{8,12},{12,8},{9,1... | collective-permute-start | bytes 3145736 | tf_op jit(solution)/shard_map/ppermute | solution.py:320
  51.3 1.0 copy-start.3
  58.1 2.1 %collective-permute-start.1 = (f32[256,512]{1,0:T(8,128)}, f32[256,512]{1,0:T(8,128)S(1)}, u32[]{:S(2)}, u32[]{:S(2)}) collective-permute-start(f32[256,512]{1,0:T(8,128)} %get-tuple-element.21), channel_id=1, source_target_pairs={{0,4},{4,0},{1,5},{5,1},{2,6},{6,2},{3,7},{7,3},{8,12},{12,8},{9,1... | collective-permute-start | bytes 1572872 | tf_op jit(solution)/shard_map/ppermute | solution.py:322
  96.3 13.5 %copy-start.1 = (bf16[32,8,512]{2,1,0:T(8,128)(2,1)}, bf16[32,8,512]{2,1,0:T(8,128)(2,1)S(1)}, u32[]{:S(2)}) copy-start(bf16[32,8,512]{2,1,0:T(8,128)(2,1)S(1)} %all_to_all.22) | copy-start | bytes 786436
  96.3 1.6 %collective-permute-start.2 = (bf16[32,8,512]{2,1,0:T(8,128)(2,1)S(1)}, bf16[32,8,512]{2,1,0:T(8,128)(2,1)S(1)}, u32[]{:S(2)}, u32[]{:S(2)}) collective-permute-start(bf16[32,8,512]{2,1,0:T(8,128)(2,1)S(1)} %all_to_all.22), channel_id=1, source_target_pairs={{0,4},{4,0},{1,5},{5,1},{2,6},{6,2},{3,7},{7,3},{8,12},{12,8},{9,1... | collective-permute-start | bytes 786440 | tf_op jit(solution)/shard_map/ppermute | solution.py:329
  97.9 11.9 %copy-start.2 = (bf16[32,8,512]{2,1,0:T(8,128)(2,1)}, bf16[32,8,512]{2,1,0:T(8,128)(2,1)S(1)}, u32[]{:S(2)}) copy-start(bf16[32,8,512]{2,1,0:T(8,128)(2,1)S(1)} %collective-permute-done.2) | copy-start | bytes 786436
Sparse Core Ops, SparseCore 0:
  29.9 75.6 all-gather.1

commit v4 on v3

--- a/solution.py
+++ b/solution.py
@@ -75,7 +75,7 @@
     dv_ref[...] = sum_ref[...].astype(BF16)
 
 
-def attention_grads(queries, keys, values, head_cot, mixing, head_gain, rows=128):
+def attention_grads(queries, keys, values, head_cot, mixing, head_gain, rows=384):
     length, cols = queries.shape
     heads = mixing.shape[0]
     width = cols // heads
@@ -161,7 +161,7 @@
         send_ref[...] = jnp.where(low, odd, even)
 
 
-def project(scale, core, mine, other, inputs, d_query, d_value, each=2):
+def project(scale, core, mine, other, inputs, d_query, d_value, each=4):
     xs, zs, rows, width = mine.shape
     length, depth = inputs.shape
     cols = d_query.shape[1]
@@ -239,19 +239,21 @@
     copy_ref[...] = (weight_ref[...].astype(F32) - rows_ref[...]).astype(BF16)
 
 
-def update(core, rate, own_factors, mine, other, moments_mine, moments_other, whole_weights):
+def update(
+    core, rate, own_factors, mine, other, moments_mine, moments_other, whole_weights, steps=2
+):
     xs, zs, rows, width = mine.shape
     rank, cols = moments_mine.shape
     maps = width // rank
     each = maps * cols // 128
-    span = 2 * xs * rows
-    depth = span * zs
+    depth = 2 * xs * rows * zs
+    span = depth // steps
     own_depth = own_factors.shape[0]
-    block = pl.BlockSpec((xs, 1, rows, width), lambda i: (0, i, 0, 0))
+    block = pl.BlockSpec((xs, zs // steps, rows, width), lambda i: (0, i, 0, 0))
     moment_block = pl.BlockSpec((rank, cols), lambda i: (0, 0))
     return pl.pallas_call(
         update_kernel,
-        grid=(zs,),
+        grid=(steps,),
         in_specs=[
             pl.BlockSpec(memory_space=pltpu.SMEM),
             pl.BlockSpec(memory_space=pltpu.SMEM),
@@ -311,9 +313,8 @@
     rank = rank_here * fs_count
     core = lax.axis_index(CORE).reshape(1)
     own_factors = factors.reshape(-1, maps * rank)
+    whole_weights = lax.all_gather(as_rows(weights).astype(BF16), FS, axis=0, tiled=True)
     columns = sent_to_all(own_factors, DEEP)
-    columns, weights = lax.optimization_barrier((columns, weights))
-    whole_weights = lax.all_gather(as_rows(weights).astype(BF16), FS, axis=0, tiled=True)
     mine = sent_to_all(columns, WIDE)
     d_query, d_value = attention_grads(queries, keys, values, head_cot, mixing, head_gain)
     mine, d_query, d_value = lax.optimization_barrier((mine, d_query, d_value))
@@ -329,8 +330,12 @@
     moments_other = lax.ppermute(moments_mine, CORE, SWAP)
     squares = moments_mine.astype(F32) ** 2 + moments_other.astype(F32) ** 2
     squares = jnp.sum(squares.reshape(planes, maps, rank_here, cols), axis=(0, 2, 3))
-    totals = lax.psum(squares, "tp")
-    rate = RATE_BASE / jnp.sqrt(1.0 + totals / (rank * cols * lax.axis_size("tp")))
+    groups = lax.axis_size("tp")
+    totals = squares
+    for distance in range(1, groups):
+        turn = [(i, (i + distance) % groups) for i in range(groups)]
+        totals = totals + lax.ppermute(squares, "tp", turn)
+    rate = RATE_BASE / jnp.sqrt(1.0 + totals / (rank * cols * groups))
     step, copies = update(
         core,
         rate,

time: 127 us -> 121 us (0.953)
  blocking collectives: 65.2 us -> 55.9 us
  Pallas kernels: 27.6 us -> 19.1 us
  waiting for transfers between devices: 6.22 us -> 13.7 us
  starting transfers between devices: 5.1 us -> 9.57 us
    psum x1 -> x0, blocking collectives: 10.3 us -> none  [per_device(): totals = lax.psum(squares, 'tp')]
    pallas_call x1, Pallas kernels: 12.8 us -> 7.99 us  [attention_grads(): pl.pallas_call(functools.partial(attention_kernel, rows), grid=(heads,),...]
    ppermute x0 -> x3, starting transfers between devices: none -> 4.57 us  [per_device(): totals = totals + lax.ppermute(squares, 'tp', turn)]
    all_to_all x1, waiting for transfers between devices: 0.01 us -> 4.32 us  [sent_to_all(): return lax.all_to_all(copies, axis, split_axis=0, concat_axis=0, tiled=True)]
    ppermute x0 -> x3, waiting for transfers between devices: none -> 3.84 us  [per_device(): totals = totals + lax.ppermute(squares, 'tp', turn)]
    all_to_all x1, blocking collectives: 16.3 us -> 19.5 us  [per_device(): parts = lax.all_to_all(summed, PLANE, 0, 0, tiled=True)]
    pallas_call x1, Pallas kernels: 8.95 us -> 6.3 us  [update(): pl.pallas_call(update_kernel, grid=(steps,), in_specs=[pl.BlockSpec(memor...]
    all_to_all x2, blocking collectives: 38.7 us -> 36.4 us  [sent_to_all(): return lax.all_to_all(copies, axis, split_axis=0, concat_axis=0, tiled=True)]
  transfers between devices with their start and end apart: 5 -> 8, of which waited for: 3 -> 6; matrix products, arithmetic and copies ran while one was open for 3% -> 4% of each run, Pallas kernels for 15% -> 11%
where the time goes in v4:
time: 121 us; the launch traced here: 120 us
  blocking collectives  55.9 us (46%)
  Pallas kernels  19.1 us (16%)
  between operations  14.1 us (12%)
  waiting for transfers between devices  13.7 us (11%)
  starting transfers between devices  9.57 us (8%)
  other arithmetic  3.68 us (3%)
  local copies, waits for them, and re-layouts  3.66 us (3%)
    all_to_all x2, blocking collectives, sent_to_all(): return lax.all_to_all(copies, axis, split_axis=0, concat_axis=0, tiled=True)  36.4 us
    all_to_all x1, blocking collectives, per_device(): parts = lax.all_to_all(summed, PLANE, 0, 0, tiled=True)  19.5 us
    pallas_call x1, Pallas kernels, attention_grads(): pl.pallas_call(functools.partial(attention_kernel, rows), grid=(heads,),...  7.99 us
    pallas_call x1, Pallas kernels, update(): pl.pallas_call(update_kernel, grid=(steps,), in_specs=[pl.BlockSpec(memor...  6.3 us
    all_to_all x1, starting transfers between devices, sent_to_all(): return lax.all_to_all(copies, axis, split_axis=0, concat_axis=0, tiled=True)  4.82 us
    pallas_call x1, Pallas kernels, project(): pl.pallas_call(functools.partial(project_kernel, scale), grid=(zs // each...  4.77 us
    ppermute x3, starting transfers between devices, per_device(): totals = totals + lax.ppermute(squares, 'tp', turn)  4.57 us
    all_to_all x1, waiting for transfers between devices, sent_to_all(): return lax.all_to_all(copies, axis, split_axis=0, concat_axis=0, tiled=True)  4.32 us
  transfers between devices with their start and end apart: 8, of which 6 were waited for; matrix products, arithmetic and copies ran while one was open for 4% of the time, Pallas kernels for 11%

profile of v4, /device:TPU:2, one launch (start us, length us, event | category | flops | bytes accessed | tf_op | source)
XLA Modules:
  0.0 119.6 jit_solution(491568783152666473)
XLA Ops:
  7.2 0.0 all-gather.2.cloned.1.call-start
  7.2 1.6 %convert_element_type.32 = bf16[32,2,512]{2,1,0:T(2,128)(2,1)} convert(f32[32,2,512]{2,1,0:T(2,128)} %param.19) | non-fusion elementwise | flops 32768 | bytes 196608 | tf_op jit(solution)/shard_map/convert_element_type | solution.py:316
  8.8 0.0 all-gather.2.cloned.1.call-update
  8.8 0.8 copy.21
  9.6 0.0 copy-start.4
  9.6 20.1 %all_to_all.20 = bf16[8,32,512]{2,1,0:T(8,128)(2,1)S(1)} all-to-all(bf16[8,32,512]{2,1,0:T(8,128)(2,1)S(1)} %broadcast_in_dim.9), channel_id=1, replica_groups=mesh['fs_0'=8,'fs_1'=4,'fs_2'=2,'tp'=4] {'fs_0'}, dimensions={0} | all-to-all | bytes 524288 | tf_op jit(solution)/shard_map/all_to_all | solution.py:302
  29.7 1.1 broadcast_in_dim.10
  30.8 4.8 %all-to-all-start.1 = ((bf16[4,8,32,512]{3,2,1,0:T(8,128)(2,1)}), bf16[4,8,32,512]{3,2,1,0:T(8,128)(2,1)S(1)}, u32[]{:S(2)}, u32[]{:S(2)}) async-start(bf16[4,8,32,512]{3,2,1,0:T(8,128)(2,1)} %broadcast_in_dim.10), calls=%async_computation.1 | async-start | bytes 2097152 | tf_op jit(solution)/shard_map/all_to_all | solution.py:302
  35.7 8.0 %attention_grads.1 = (bf16[384,512]{1,0:T(8,128)(2,1)}, bf16[384,512]{1,0:T(8,128)(2,1)}) custom-call(f32[4]{0:T(128)} %mix_ref.1, bf16[384,512]{1,0:T(8,128)(2,1)} %q_ref.1, bf16[384,512]{1,0:T(8,128)(2,1)} %k_ref.1, bf16[384,512]{1,0:T(8,128)(2,1)} %v_ref.1, bf16[384,512]{1,0:T(8,128)(2,1)} %up_ref.1, f32[1,128]{1,0:T(1,128)} %bitcast.36), custom_call_target="tpu_custom_call" | custom-call | flops 1509949440 | bytes 2359296 | tf_op jit(solution)/shard_map/attention_grads/pallas_call | solution.py:83
  43.7 0.0 copy-done.4
  43.7 0.0 copy-start.5
  43.7 4.3 %all-to-all-done.1.mine_ref = bf16[4,8,32,512]{3,2,1,0:T(8,128)(2,1)S(1)} async-done(((bf16[4,8,32,512]{3,2,1,0:T(8,128)(2,1)}), bf16[4,8,32,512]{3,2,1,0:T(8,128)(2,1)S(1)}, u32[]{:S(2)}, u32[]{:S(2)}) %all-to-all-start.1) | async-done | bytes 1048608 | tf_op jit(solution)/shard_map/all_to_all | solution.py:302
  48.0 0.0 copy-start
  48.0 0.0 collective-permute-start
  48.0 2.7 %collective-permute-done.other_ref = bf16[4,8,32,512]{3,2,1,0:T(8,128)(2,1)S(1)} collective-permute-done((bf16[4,8,32,512]{3,2,1,0:T(8,128)(2,1)S(1)}, bf16[4,8,32,512]{3,2,1,0:T(8,128)(2,1)S(1)}, u32[]{:S(2)}, u32[]{:S(2)}) %collective-permute-start) | collective-permute-done | bytes 1048608 | tf_op jit(solution)/shard_map/ppermute | solution.py:321
  50.7 0.0 copy-start.3
  50.7 0.0 copy-done
  50.7 1.0 copy-done.3
  51.6 4.8 %project.1 = (f32[256,512]{1,0:T(8,128)}, f32[256,512]{1,0:T(8,128)}) custom-call(s32[1]{0:T(128)} %bitcast.core_ref, bf16[4,8,32,512]{3,2,1,0:T(8,128)(2,1)} %copy-done, bf16[4,8,32,512]{3,2,1,0:T(8,128)(2,1)} %copy-done.3, bf16[384,2048]{1,0:T(8,128)(2,1)} %in_ref.1, bf16[384,512]{1,0:T(8,128)(2,1)} %get-tuple-element.15.dq_ref, ...), custom_call_target="tpu_custom_call" | custom-call | flops 1207959552 | bytes 5505024 | tf_op jit(solution)/shard_map/project/pallas_call | solution.py:173
  56.4 0.1 collective-permute-start.1
  56.6 2.0 %collective-permute-done.1 = f32[256,512]{1,0:T(8,128)S(1)} collective-permute-done((f32[256,512]{1,0:T(8,128)}, f32[256,512]{1,0:T(8,128)S(1)}, u32[]{:S(2)}, u32[]{:S(2)}) %collective-permute-start.1) | collective-permute-done | bytes 524320 | tf_op jit(solution)/shard_map/ppermute | solution.py:323
  58.5 1.1 fusion
  59.7 19.5 %all_to_all.21 = bf16[32,8,512]{2,1,0:T(8,128)(2,1)S(1)} all-to-all(bf16[32,8,512]{2,1,0:T(8,128)(2,1)S(1)} %fusion), channel_id=1, replica_groups=mesh['fs_0'=8,'fs_1'=4,'fs_2'=2,'tp'=4] {'fs_0','fs_1'}, dimensions={0} | all-to-all | bytes 524288 | tf_op jit(solution)/shard_map/all_to_all | solution.py:325
  79.2 0.0 copy-done.5
  79.3 16.2 %all_to_all.22 = bf16[32,8,512]{2,1,0:T(8,128)(2,1)S(1)} all-to-all(bf16[32,8,512]{2,1,0:T(8,128)(2,1)S(1)} %broadcast_in_dim.11), channel_id=1, replica_groups=mesh['fs_0'=8,'fs_1'=4,'fs_2'=2,'tp'=4] {'fs_0','fs_1'}, dimensions={0} | all-to-all | bytes 524288 | tf_op jit(solution)/shard_map/all_to_all | solution.py:302
  95.5 0.0 copy-start.1
  95.5 0.0 collective-permute-start.2
  95.5 0.7 copy.20
  96.2 0.9 collective-permute-done.2
  97.1 0.0 copy-start.2
  97.1 0.2 add_reduce_fusion
  97.3 0.1 reduce_sum.27
  97.4 0.1 reduce_sum.28
  97.5 3.0 %collective-permute-start.5 = (f32[2]{0:T(128)S(1)}, f32[2]{0:T(128)S(1)}, u32[]{:S(2)}, u32[]{:S(2)}) collective-permute-start(f32[2]{0:T(128)S(1)} %reduce_sum.28), channel_id=1, source_target_pairs={{0,3},{1,0},{2,1},{3,2},{4,7},{5,4},{6,5},{7,6},{8,11},{9,8},{10,9... | collective-permute-start | bytes 32 | tf_op jit(solution)/shard_map/ppermute | solution.py:337
  100.5 0.6 collective-permute-start.4
  101.2 0.9 collective-permute-start.3
  102.1 0.0 collective-permute-done.5
  102.1 3.5 %collective-permute-done.4 = f32[2]{0:T(128)S(1)} collective-permute-done((f32[2]{0:T(128)S(1)}, f32[2]{0:T(128)S(1)}, u32[]{:S(2)}, u32[]{:S(2)}) %collective-permute-start.4) | collective-permute-done | bytes 40 | tf_op jit(solution)/shard_map/ppermute | solution.py:337
  105.6 0.3 collective-permute-done.3
  105.9 0.5 rsqrt_multiply_fusion.scale_ref
  106.5 0.0 all-gather.2.cloned.1.call-done.weight_ref
  106.5 0.0 copy-done.1
  106.5 0.0 copy-done.2
  106.5 6.3 %low_rank_update.1 = (f32[256,128]{1,0:T(8,128)}, bf16[16384,128]{1,0:T(8,128)(2,1)}) custom-call(s32[1]{0:T(128)} %bitcast.core_ref, f32[2]{0:T(128)} %rsqrt_multiply_fusion.scale_ref, bf16[32,512]{1,0:T(8,128)(2,1)} %bitcast.31, bf16[4,8,32,512]{3,2,1,0:T(8,128)(2,1)} %copy-done, bf16[4,8,32,512]{3,2,1,0:T(8,128)(2,1)} %copy-done.3, ...), custom_call_target="tpu_custom_call" | custom-call | flops 1073741824 | bytes 10485760 | tf_op jit(solution)/shard_map/low_rank_update/pallas_call | solution.py:254
  (6 shorter events, 0.1 us)
Async XLA Ops:
  7.2 99.3 %all-gather.2.cloned.1.call-start = ((), (), s32[]{:S(2)}) async-start(), calls=%async_computation.4 | async-start | bytes 4259840 | tf_op jit(solution)/shard_map/all_gather | solution.py:316
  9.6 34.1 %copy-start.4 = (bf16[4,8,2,256]{3,1,2,0:T(8,128)(2,1)}, bf16[4,8,2,256]{3,1,2,0:T(8,128)(2,1)S(1)}, u32[]{:S(2)}) copy-start(bf16[4,8,2,256]{3,1,2,0:T(8,128)(2,1)S(1)} %copy.21) | copy-start | bytes 98308
  30.8 17.2 %all-to-all-start.1 = ((bf16[4,8,32,512]{3,2,1,0:T(8,128)(2,1)}), bf16[4,8,32,512]{3,2,1,0:T(8,128)(2,1)S(1)}, u32[]{:S(2)}, u32[]{:S(2)}) async-start(bf16[4,8,32,512]{3,2,1,0:T(8,128)(2,1)} %broadcast_in_dim.10), calls=%async_computation.1 | async-start | bytes 2097152 | tf_op jit(solution)/shard_map/all_to_all | solution.py:302
  43.7 35.6 %copy-start.5 = (f32[4,2,512]{2,1,0:T(2,128)S(1)}, f32[4,2,512]{2,1,0:T(2,128)}, u32[]{:S(2)}) copy-start(f32[4,2,512]{2,1,0:T(2,128)} %param.18) | copy-start | bytes 49156
  48.0 2.7 %copy-start = (bf16[4,8,32,512]{3,2,1,0:T(8,128)(2,1)}, bf16[4,8,32,512]{3,2,1,0:T(8,128)(2,1)S(1)}, u32[]{:S(2)}) copy-start(bf16[4,8,32,512]{3,2,1,0:T(8,128)(2,1)S(1)} %all-to-all-done.1.mine_ref) | copy-start | bytes 3145732
  48.0 2.7 %collective-permute-start = (bf16[4,8,32,512]{3,2,1,0:T(8,128)(2,1)S(1)}, bf16[4,8,32,512]{3,2,1,0:T(8,128)(2,1)S(1)}, u32[]{:S(2)}, u32[]{:S(2)}) collective-permute-start(bf16[4,8,32,512]{3,2,1,0:T(8,128)(2,1)S(1)} %all-to-all-done.1.mine_ref), channel_id=1, source_target_pairs={{0,4},{4,0},{1,5},{5,1},{2,6},{6,2},{3,7},{7,3},{8,12},{12,8},{9,1... | collective-permute-start | bytes 3145736 | tf_op jit(solution)/shard_map/ppermute | solution.py:321
  50.7 1.0 copy-start.3
  56.4 2.1 %collective-permute-start.1 = (f32[256,512]{1,0:T(8,128)}, f32[256,512]{1,0:T(8,128)S(1)}, u32[]{:S(2)}, u32[]{:S(2)}) collective-permute-start(f32[256,512]{1,0:T(8,128)} %get-tuple-element.18), channel_id=1, source_target_pairs={{0,4},{4,0},{1,5},{5,1},{2,6},{6,2},{3,7},{7,3},{8,12},{12,8},{9,1... | collective-permute-start | bytes 1572872 | tf_op jit(solution)/shard_map/ppermute | solution.py:323
  95.5 11.0 %copy-start.1 = (bf16[32,8,512]{2,1,0:T(8,128)(2,1)}, bf16[32,8,512]{2,1,0:T(8,128)(2,1)S(1)}, u32[]{:S(2)}) copy-start(bf16[32,8,512]{2,1,0:T(8,128)(2,1)S(1)} %all_to_all.22) | copy-start | bytes 786436
  95.5 1.5 %collective-permute-start.2 = (bf16[32,8,512]{2,1,0:T(8,128)(2,1)S(1)}, bf16[32,8,512]{2,1,0:T(8,128)(2,1)S(1)}, u32[]{:S(2)}, u32[]{:S(2)}) collective-permute-start(bf16[32,8,512]{2,1,0:T(8,128)(2,1)S(1)} %all_to_all.22), channel_id=1, source_target_pairs={{0,4},{4,0},{1,5},{5,1},{2,6},{6,2},{3,7},{7,3},{8,12},{12,8},{9,1... | collective-permute-start | bytes 786440 | tf_op jit(solution)/shard_map/ppermute | solution.py:330
  97.1 9.4 %copy-start.2 = (bf16[32,8,512]{2,1,0:T(8,128)(2,1)}, bf16[32,8,512]{2,1,0:T(8,128)(2,1)S(1)}, u32[]{:S(2)}) copy-start(bf16[32,8,512]{2,1,0:T(8,128)(2,1)S(1)} %collective-permute-done.2) | copy-start | bytes 786436
  97.5 4.6 %collective-permute-start.5 = (f32[2]{0:T(128)S(1)}, f32[2]{0:T(128)S(1)}, u32[]{:S(2)}, u32[]{:S(2)}) collective-permute-start(f32[2]{0:T(128)S(1)} %reduce_sum.28), channel_id=1, source_target_pairs={{0,3},{1,0},{2,1},{3,2},{4,7},{5,4},{6,5},{7,6},{8,11},{9,8},{10,9... | collective-permute-start | bytes 32 | tf_op jit(solution)/shard_map/ppermute | solution.py:337
  100.5 5.1 %collective-permute-start.4 = (f32[2]{0:T(128)S(1)}, f32[2]{0:T(128)S(1)}, u32[]{:S(2)}, u32[]{:S(2)}) collective-permute-start(f32[2]{0:T(128)S(1)} %reduce_sum.28), channel_id=1, source_target_pairs={{0,2},{1,3},{2,0},{3,1},{4,6},{5,7},{6,4},{7,5},{8,10},{9,11},{10,... | collective-permute-start | bytes 32 | tf_op jit(solution)/shard_map/ppermute | solution.py:337
  101.2 4.8 %collective-permute-start.3 = (f32[2]{0:T(128)S(1)}, f32[2]{0:T(128)S(1)}, u32[]{:S(2)}, u32[]{:S(2)}) collective-permute-start(f32[2]{0:T(128)S(1)} %reduce_sum.28), channel_id=1, source_target_pairs={{0,1},{1,2},{2,3},{3,0},{4,5},{5,6},{6,7},{7,4},{8,9},{9,10},{10,1... | collective-permute-start | bytes 32 | tf_op jit(solution)/shard_map/ppermute | solution.py:337
Sparse Core Ops, SparseCore 0:
  11.3 83.1 all-gather.1
